TPU v7x, 32 devices: a whole 2x2x4 slice. The times are simulated.
32 devices in a mesh: sp: 8 (over z, x), tp: 4 (over y, core).
Axes of the slice: x: 2, y: 2, z: 4, core: 2. Of those that a mesh axis runs over, the one named last changes fastest.
Arguments:
- tokens: bfloat16 [2048, 4096], P('sp', 'tp'), may hold values from -6 to 6
- pre_gain: float32 [4096], replicated, may hold values from 0.1 to 1.9
- rate_factor: float32 [2048], P('sp'), may hold values from 0.5 to 2, as said below
- w_rec_in: bfloat16 [4096, 1024], P(None, 'tp'), may hold values from -0.09375 to 0.09375
- w_rec_gate: bfloat16 [4096, 1024], P(None, 'tp')
- conv_taps: float32 [4, 1024], P(None, 'tp'), may hold values from -3 to 3
- rate_maps: bfloat16 [8, 128, 128], P('tp'), may hold values from -0.5 to 0.5
- input_maps: bfloat16 [8, 128, 128], P('tp'), may hold values from -0.5 to 0.5
- decay_param: float32 [1024], P('tp'), as said below
- w_query: bfloat16 [4096, 1536], P(None, 'tp'), may hold values from -0.09375 to 0.09375
- w_latent: bfloat16 [4096, 512], replicated, may hold values from -0.09375 to 0.09375
- w_rope_key: bfloat16 [4096, 64], replicated, may hold values from -0.09375 to 0.09375
- latent_gain: float32 [512], replicated, may hold values from 0.7 to 100, as said below
- w_expand: bfloat16 [512, 2048], P(None, 'tp')
- rec_gain: float32 [1024], P('tp'), may hold values from 0.1 to 1.9
- att_gain: float32 [1024], P('tp'), may hold values from 0.1 to 1.9
- w_out_rec: bfloat16 [1024, 4096], P('tp'), may hold values from -0.125 to 0.125
- w_out_att: bfloat16 [1024, 4096], P('tp'), may hold values from -0.125 to 0.125
- post_gain: float32 [4096], replicated, may hold values from 0.1 to 1.9
Outputs:
- layer_out: bfloat16 [2048, 4096], P(('sp', 'tp'))
Inputs may be any that keep to these rules, and one draw needn't show every extreme that they name: `rate_factor`: one positive factor for each position. `decay_param`: one parameter for each recurrent channel. `latent_gain`: one positive gain for each latent entry.
All inputs are finite; a program needn't handle non-finite values.
Results may differ from a plain program's by a relative error of at most 0.017.
The roundings to bfloat16 on the way count: a program that leaves them out, or rounds other values in their place, can miss the bound.
Values may be sent and summed in bfloat16 or wider, within the bound.
A program may use at most 128 MiB of HBM per device.

v0:
```python
import math

import jax
import jax.numpy as jnp
from jax import lax
from jax.sharding import PartitionSpec as P

NOPE = 128
ROPE = 64
VDIM = 128


EPS = 1e-06
RATE_C = 8.0
THETA = 10000.0
span_limit = 2048


def passed_along(block, axis, distance):
    devices = range(lax.axis_size(axis))
    route = [(i - distance, i) for i in devices if i - distance in devices]
    return lax.ppermute(block, axis, route)


def entering(value, axis, join, neutral):
    count, mine = (lax.axis_size(axis), lax.axis_index(axis))
    pieces = jax.tree.map(lambda part: lax.all_gather(part, axis), value)
    subtotal = jax.tree.map(
        lambda part, zero: jnp.full_like(part, 0) + jnp.asarray(zero, part.dtype), value, neutral
    )

    def step(position, subtotal):
        longer = join(subtotal, jax.tree.map(lambda part: part[position], pieces))
        return jax.tree.map(lambda new, old: jnp.where(position < mine, new, old), longer, subtotal)

    return lax.fori_loop(0, count - 1, step, subtotal)


def rms_inverse(values):
    return lax.rsqrt(jnp.mean(values * values, axis=-1, keepdims=True) + EPS)


def rotate(values, cosine, sine_part):
    half_width = values.shape[-1] // 2
    leading = values[..., :half_width]
    trailing = values[..., half_width:]
    return jnp.concatenate(
        [leading * cosine - trailing * sine_part, trailing * cosine + leading * sine_part], axis=-1
    )


def angles(length, offset, span_width):
    frequency = 1.0 / THETA ** (jnp.arange(0, span_width, 2).astype(jnp.float32) / span_width)
    places = (offset + jnp.arange(length)).astype(jnp.float32)
    turned = places[:, None] * frequency[None, :]
    return (jnp.cos(turned), jnp.sin(turned))


def combine_steps(earlier, later):
    return (earlier[0] * later[0], later[0] * earlier[1] + later[1])


def attend_block(state_now, query_nope, query_rope, places, keys_nope, key_rope, values, key_root):
    maxima, totals, accumulated = state_now
    scaling = 1.0 / math.sqrt(query_nope.shape[-1] + query_rope.shape[-1])
    scores = jnp.einsum("qhd,khd->hqk", query_nope, keys_nope, preferred_element_type=jnp.float32)
    scores = scores + jnp.einsum(
        "qhd,kd->hqk", query_rope, key_rope, preferred_element_type=jnp.float32
    )
    scores = scores * scaling
    key_places = key_root + jnp.arange(keys_nope.shape[0])
    visible = key_places[None, :] <= places[:, None]
    scores = jnp.where(visible[None], scores, -jnp.inf)
    largest = jnp.maximum(maxima, jnp.max(scores, axis=-1))
    anchor = jnp.where(largest == -jnp.inf, 0.0, largest)
    weights = jnp.exp(scores - anchor[..., None])
    shrink = jnp.exp(maxima - anchor)
    totals = totals * shrink + jnp.sum(weights, axis=-1)
    accumulated = accumulated * shrink[..., None] + jnp.einsum(
        "hqk,khd->hqd", weights.astype(jnp.bfloat16), values, preferred_element_type=jnp.float32
    )
    return (largest, totals, accumulated)


def shards(
    tokens,
    pre_gain,
    rate_factor,
    w_rec_in,
    w_rec_gate,
    conv_taps,
    rate_maps,
    input_maps,
    decay_param,
    w_query,
    w_latent,
    w_rope_key,
    latent_gain,
    w_expand,
    rec_gain,
    att_gain,
    w_out_rec,
    w_out_att,
    post_gain,
):
    row_count = tokens.shape[0]
    model_width = w_rec_in.shape[0]
    channels = w_rec_in.shape[1]
    heads_here = w_query.shape[1] // (NOPE + ROPE)
    group_size = lax.axis_size("tp")
    first_place = lax.axis_index("sp") * row_count
    places = first_place + jnp.arange(row_count)
    last_place = first_place + row_count - 1
    piece_wide = lax.all_gather(tokens, "tp", axis=1, tiled=True).astype(jnp.float32)
    piece_low = (piece_wide * pre_gain).astype(jnp.bfloat16)

    def accumulate(source, weight):
        return jnp.dot(source, weight, preferred_element_type=jnp.float32)

    squares = jnp.sum(piece_wide * piece_wide, axis=1, keepdims=True)
    sum_input = accumulate(piece_low, w_rec_in)
    sum_gate = accumulate(piece_low, w_rec_gate)
    sum_query = accumulate(piece_low, w_query)
    sum_latent = accumulate(piece_low, w_latent)
    sum_rope = accumulate(piece_low, w_rope_key)
    inverse = lax.rsqrt(squares / model_width + EPS)
    rec_input = (inverse * sum_input).astype(jnp.bfloat16)
    gate_value = inverse * sum_gate
    query_raw = inverse * sum_query
    latent_raw = inverse * sum_latent
    rope_raw = inverse * sum_rope
    taps = conv_taps.shape[0]
    tail_rows = rec_input[row_count - (taps - 1) :]
    before = passed_along(tail_rows, "sp", 1)
    padded = jnp.concatenate([before, rec_input], axis=0)
    convolved = conv_taps[0] * padded[0:row_count].astype(jnp.float32)
    for tap_index in range(1, taps):
        convolved = convolved + conv_taps[tap_index] * padded[
            tap_index : tap_index + row_count
        ].astype(jnp.float32)
    conv_low = convolved.astype(jnp.bfloat16)
    blocks = conv_low.reshape(row_count, rate_maps.shape[0], rate_maps.shape[1])
    rate_gate = jax.nn.sigmoid(
        jnp.einsum("sbi,bij->sbj", blocks, rate_maps, preferred_element_type=jnp.float32)
    ).reshape(row_count, channels)
    entry_gate = jax.nn.sigmoid(
        jnp.einsum("sbi,bij->sbj", blocks, input_maps, preferred_element_type=jnp.float32)
    ).reshape(row_count, channels)
    log_keep = -RATE_C * rate_factor[:, None] * rate_gate * jax.nn.softplus(-decay_param)
    keep_rate = jnp.exp(log_keep)
    driven = jnp.sqrt(-jnp.expm1(2.0 * log_keep)) * entry_gate * convolved
    cum_keep, local_state = lax.associative_scan(combine_steps, (keep_rate, driven), axis=0)
    identity = (jnp.ones((channels,), jnp.float32), jnp.zeros((channels,), jnp.float32))
    chain_keep, carried = entering(
        (cum_keep[row_count - 1], local_state[row_count - 1]), "sp", combine_steps, identity
    )
    state_seq = local_state + cum_keep * carried[None, :]
    rec_out = state_seq * jax.nn.gelu(gate_value)
    rec_squares = jnp.sum(rec_out * rec_out, axis=1, keepdims=True)
    cosine, sine_part = angles(row_count, first_place, ROPE)
    query_heads = query_raw.reshape(row_count, heads_here, NOPE + ROPE)
    query_nope = query_heads[:, :, :NOPE].astype(jnp.bfloat16)
    query_rope = rotate(query_heads[:, :, NOPE:], cosine[:, None, :], sine_part[:, None, :]).astype(
        jnp.bfloat16
    )
    own_latent = (latent_raw * rms_inverse(latent_raw) * latent_gain).astype(jnp.bfloat16)
    rope_key = rotate(rope_raw, cosine, sine_part).astype(jnp.bfloat16)
    start_state = (
        jnp.full((heads_here, row_count), -jnp.inf, jnp.float32),
        jnp.zeros((heads_here, row_count), jnp.float32),
        jnp.zeros((heads_here, row_count, VDIM), jnp.float32),
    )
    expanded_local = jnp.dot(own_latent, w_expand, preferred_element_type=jnp.float32).astype(
        jnp.bfloat16
    )
    key_source = lax.all_gather(expanded_local, "sp", axis=0, tiled=True)
    rope_source = lax.all_gather(rope_key, "sp", axis=0, tiled=True)
    total_rows = key_source.shape[0]
    key_span = math.gcd(total_rows, span_limit)

    def one_span(span_index, state_inner):
        key_root = span_index * key_span

        def compute(state_deep):
            source_rows = lax.dynamic_slice_in_dim(key_source, span_index * key_span, key_span, 0)
            rope_rows = lax.dynamic_slice_in_dim(rope_source, span_index * key_span, key_span, 0)
            expanded = source_rows
            expanded = expanded.reshape(key_span, heads_here, NOPE + VDIM)
            return attend_block(
                state_deep,
                query_nope,
                query_rope,
                places,
                expanded[:, :, :NOPE],
                rope_rows,
                expanded[:, :, NOPE:],
                key_root,
            )

        def keep_state(state_deep):
            return state_deep

        return lax.cond(key_root <= last_place, compute, keep_state, state_inner)

    maxima, totals, accumulated = lax.fori_loop(0, total_rows // key_span, one_span, start_state)
    att_out = (
        (accumulated / totals[..., None]).transpose(1, 0, 2).reshape(row_count, heads_here * VDIM)
    )
    att_squares = jnp.sum(att_out * att_out, axis=1, keepdims=True)
    rec_total, att_total = lax.psum((rec_squares, att_squares), "tp")
    rec_norm = (rec_out * lax.rsqrt(rec_total / (channels * group_size) + EPS) * rec_gain).astype(
        jnp.bfloat16
    )
    att_norm = (
        att_out * lax.rsqrt(att_total / (heads_here * VDIM * group_size) + EPS) * att_gain
    ).astype(jnp.bfloat16)
    mixed_sum = lax.psum_scatter(
        (
            jnp.dot(rec_norm, w_out_rec, preferred_element_type=jnp.float32)
            + jnp.dot(att_norm, w_out_att, preferred_element_type=jnp.float32)
        ).astype(jnp.bfloat16),
        "tp",
        scatter_dimension=0,
        tiled=True,
    ).astype(jnp.float32)
    return (mixed_sum * rms_inverse(mixed_sum) * post_gain).astype(jnp.bfloat16)


def solution(mesh):
    placed = (
        P("sp", "tp"),
        P(),
        P("sp"),
        P(None, "tp"),
        P(None, "tp"),
        P(None, "tp"),
        P("tp", None, None),
        P("tp", None, None),
        P("tp"),
        P(None, "tp"),
        P(),
        P(),
        P(),
        P(None, "tp"),
        P("tp"),
        P("tp"),
        P("tp", None),
        P("tp", None),
        P(),
    )
    return jax.shard_map(
        shards, mesh=mesh, in_specs=placed, out_specs=P(("sp", "tp"), None), check_vma=False
    )
```

profile of v0, /device:TPU:0, one launch (start us, length us, event | category | flops | bytes accessed | tf_op | source)
XLA Modules:
  0.0 334.9 jit_solution(9606723761074546730)
XLA Ops:
  11.2 23.0 %all-gather.5.cloned.1.call-done = bf16[256,4096]{1,0:T(8,128)(2,1)} async-done(((bf16[256,1024]{1,0:T(8,128)(2,1)}), bf16[256,4096]{1,0:T(8,128)(2,1)}) %all-gather.5.cloned.1.call-update) | async-done | bytes 2097168 | tf_op jit(solution)/shard_map/all_gather | solution.py:114
  34.2 2.2 fusion.15
  36.5 2.5 fusion.23
  39.6 4.1 %collective-permute-start = (bf16[3,256]{1,0:T(4,128)(2,1)}, bf16[3,256]{1,0:T(4,128)(2,1)}, u32[]{:S(2)}, u32[]{:S(2)}) collective-permute-start(bf16[3,256]{1,0:T(4,128)(2,1)} %slice.384), channel_id=1, source_target_pairs={{0,4},{4,8},{8,12},{12,16},{16,20},{20,24},{24,28},{1,5},{5,9},{9,... | collective-permute-start | bytes 4616 | tf_op jit(solution)/shard_map/ppermute | solution.py:22
  46.3 3.6 %convolution_multiply_fusion.1 = f32[256,384]{1,0:T(8,128)} fusion(bf16[4096,384]{1,0:T(8,128)(2,1)S(1)} %copy-done, bf16[256,4096]{1,0:T(8,128)(2,1)} %all-gather.5.cloned.1.call-done, f32[4096]{0:T(1024)} %param.24, f32[256]{0:T(256)} %copy-done.20), kind=kOutput, calls=%fused_computation.32 | convolution fusion | flops 808550400 | bytes 5653504 | tf_op jit(solution)/shard_map/dot_general | solution.py:118
  51.8 2.6 convolution_multiply_fusion.4
  54.6 33.6 %all_gather.19 = bf16[2048,64]{0,1:T(8,128)(2,1)} all-gather(bf16[256,64]{0,1:T(8,128)(2,1)S(1)} %pad_maximum_fusion.8), channel_id=1, replica_groups=mesh['sp'=8,'tp'=4] {'sp'}, dimensions={0}, use_global_device_ids=true | all-gather | bytes 294912 | tf_op jit(solution)/shard_map/all_gather | solution.py:177
  98.5 2.2 multiply_multiply_fusion.1
  199.9 2.0 pad.124
  207.9 2.2 pad.127
  211.7 2.3 pad.129
  214.0 2.2 pad.111
  217.6 2.1 pad.110
  225.5 17.7 %all-gather = f32[8,1,256]{2,1,0:T(1,128)S(1)} all-gather(f32[1,1,256]{2,1,0:T(1,128)S(1)} %add_bitcast_fusion.1), channel_id=1, replica_groups=mesh['sp'=8,'tp'=4] {'sp'}, dimensions={0}, use_global_device_ids=true | all-gather | bytes 9216 | tf_op jit(solution)/shard_map/all_gather | solution.py:27
  243.2 2.3 pad.113
  248.7 17.0 %all-gather.1 = f32[8,1,256]{2,1,0:T(1,128)S(1)} all-gather(f32[1,1,256]{2,1,0:T(1,128)S(1)} %add_bitcast_fusion), channel_id=1, replica_groups=mesh['sp'=8,'tp'=4] {'sp'}, dimensions={0}, use_global_device_ids=true | all-gather | bytes 9216 | tf_op jit(solution)/shard_map/all_gather | solution.py:27
  266.1 4.0 %multiply_reduce_fusion.1 = (f32[256]{0:T(256)S(1)}, f32[256,256]{1,0:T(8,128)}) fusion(bf16[4096,256]{1,0:T(8,128)(2,1)} %param.27, bf16[256,4096]{1,0:T(8,128)(2,1)} %all-gather.5.cloned.1.call-done, f32[4096]{0:T(1024)} %param.24, f32[256]{0:T(256)} %copy-done.20, f32[256]{0:T(256)S(1)} %get-tuple-element.224, f32[256,256]{1,0:T(8,128)} %pad.128, ...), kind=kOutput, calls=%fused_computation.67 | convolution fusion | flops 541064960 | bytes 5524480 | tf_op jit(solution)/shard_map/dot_general | solution.py:118
  270.1 14.6 %conditional.1 = (f32[2,256]{1,0:T(2,128)S(1)}, f32[2,256,128]{1,2,0:T(8,128)}) conditional(s32[]{:T(128)} %convert_element_type.81, (f32[2,256]{1,0:T(2,128)S(1)}, f32[2,256,128]{2,1,0:T(8,128)S(1)}) %tuple.113, (s32[]{:T(128)}, s32[256]{0:T(256)S(1)}, bf16[2048,512]{1,0:T(8,128)(2,1)}, f32[256,2,192]{0,2,1:T(8,128)}, bf16[2048,64]{0,1:T(8,128)(2,1)}, ...), branch_computations={%region_6.7_spmd, %region_7.10_spmd} | conditional | flops 680135424 | bytes 39873612 | solution.py:203
  270.1 4.0 %copy.56 = bf16[2048,512]{0,1:T(8,128)(2,1)} copy(bf16[2048,512]{1,0:T(8,128)(2,1)} %get-tuple-element.265) | data formatting | bytes 4194304 | tf_op jit(solution)/shard_map
  276.0 2.0 fusion.11
  285.7 5.7 %all-reduce.32 = (f32[256,1]{0,1:T(1,128)S(1)}, f32[256,1]{0,1:T(1,128)S(1)}) all-reduce(f32[256,1]{0,1:T(1,128)S(1)} %bitcast.90, f32[256,1]{0,1:T(1,128)S(1)} %bitcast.84), channel_id=1, replica_groups=mesh['sp'=8,'tp'=4] {'tp'}, use_global_device_ids=true, to_apply=%region_4.5 | all-reduce | flops 512 | bytes 4096 | tf_op jit(solution)/shard_map/psum | solution.py:210
  291.5 2.6 fusion.52
  294.1 2.1 fusion.14
  296.2 28.9 %reduce-scatter.2.cloned.1.call-done = bf16[64,4096]{1,0:T(8,128)(2,1)} async-done(((bf16[256,4096]{1,0:T(8,128)(2,1)}), bf16[64,4096]{1,0:T(8,128)(2,1)}) %reduce-scatter.2.cloned.1.call-update) | async-done | bytes 524304 | tf_op jit(solution)/shard_map/reduce_scatter | solution.py:217
  (233 shorter events, 150.5 us)
Async XLA Ops:
  6.5 39.7 %copy-start = (bf16[4096,384]{1,0:T(8,128)(2,1)S(1)}, bf16[4096,384]{1,0:T(8,128)(2,1)}, u32[]{:S(2)}) copy-start(bf16[4096,384]{1,0:T(8,128)(2,1)} %param.32) | copy-start | bytes 9437188
  6.5 27.7 %all-gather.5.cloned.1.call-start = ((), (), s32[]{:S(2)}) async-start(), calls=%async_computation.1 | async-start | bytes 2621440 | tf_op jit(solution)/shard_map/all_gather | solution.py:114
  7.3 262.8 %all-gather.7.cloned.1.call-start = ((), (), s32[]{:S(2)}) async-start(), calls=%async_computation.2 | async-start | bytes 2359296 | tf_op jit(solution)/shard_map/all_gather | solution.py:176
  36.5 7.2 %copy-start.20 = (f32[256]{0:T(256)}, f32[256]{0:T(256)S(1)}, u32[]{:S(2)}) copy-start(f32[256]{0:T(256)S(1)} %add_rsqrt_fusion.3) | copy-start | bytes 3076
  36.5 7.2 %copy-start.22 = (bf16[4096,512]{1,0:T(8,128)(2,1)S(1)}, bf16[4096,512]{1,0:T(8,128)(2,1)}, u32[]{:S(2)}) copy-start(bf16[4096,512]{1,0:T(8,128)(2,1)} %param.33) | copy-start | bytes 12582916
  36.5 7.2 %copy-start.24 = (f32[4096]{0:T(1024)S(1)}, f32[4096]{0:T(1024)}, u32[]{:S(2)}) copy-start(f32[4096]{0:T(1024)} %param.24) | copy-start | bytes 49156
  39.6 5.5 %copy-start.5 = (bf16[512,512]{1,0:T(8,128)(2,1)S(1)}, bf16[512,512]{1,0:T(8,128)(2,1)}, u32[]{:S(2)}) copy-start(bf16[512,512]{1,0:T(8,128)(2,1)} %param.36) | copy-start | bytes 1572868
  39.6 5.5 %copy-start.17 = (f32[512]{0:T(512)S(1)}, f32[512]{0:T(512)}, u32[]{:S(2)}) copy-start(f32[512]{0:T(512)} %param.35) | copy-start | bytes 6148
  39.6 50.2 %collective-permute-start = (bf16[3,256]{1,0:T(4,128)(2,1)}, bf16[3,256]{1,0:T(4,128)(2,1)}, u32[]{:S(2)}, u32[]{:S(2)}) collective-permute-start(bf16[3,256]{1,0:T(4,128)(2,1)} %slice.384), channel_id=1, source_target_pairs={{0,4},{4,8},{8,12},{12,16},{16,20},{20,24},{24,28},{1,5},{5,9},{9,... | collective-permute-start | bytes 4616 | tf_op jit(solution)/shard_map/ppermute | solution.py:22
  46.2 278.9 %reduce-scatter.2.cloned.1.call-start = ((), (), s32[]{:S(2)}) async-start(), calls=%async_computation.3 | async-start | bytes 2621440 | tf_op jit(solution)/shard_map/reduce_scatter | solution.py:217
  51.8 2.6 copy-start.19
  51.8 2.6 copy-start.21
  51.8 38.0 %copy-start.15 = (f32[1,256]{1,0:T(1,128)S(1)}, f32[1,256]{1,0:T(1,128)}, u32[]{:S(2)}) copy-start(f32[1,256]{1,0:T(1,128)} %get-tuple-element.332) | copy-start | bytes 3076
  51.8 38.0 %copy-start.16 = (f32[1,256]{1,0:T(1,128)S(1)}, f32[1,256]{1,0:T(1,128)}, u32[]{:S(2)}) copy-start(f32[1,256]{1,0:T(1,128)} %get-tuple-element.333) | copy-start | bytes 3076
  51.8 40.3 %copy-start.23 = (bf16[2,128,128]{2,1,0:T(8,128)(2,1)S(1)}, bf16[2,128,128]{2,1,0:T(8,128)(2,1)}, u32[]{:S(2)}) copy-start(bf16[2,128,128]{2,1,0:T(8,128)(2,1)} %param.30) | copy-start | bytes 196612
  191.6 24.5 %copy-start.14 = (f32[1,256]{1,0:T(1,128)S(1)}, f32[1,256]{1,0:T(1,128)}, u32[]{:S(2)}) copy-start(f32[1,256]{1,0:T(1,128)} %slice.390) | copy-start | bytes 3076
  202.0 21.3 %copy-start.13 = (f32[1,256]{1,0:T(1,128)S(1)}, f32[1,256]{1,0:T(1,128)}, u32[]{:S(2)}) copy-start(f32[1,256]{1,0:T(1,128)} %slice.415) | copy-start | bytes 3076
  207.0 38.6 %copy-start.12 = (f32[1,256]{1,0:T(1,128)S(1)}, f32[1,256]{1,0:T(1,128)}, u32[]{:S(2)}) copy-start(f32[1,256]{1,0:T(1,128)} %slice.389) | copy-start | bytes 3076
  211.7 54.0 %copy-start.8 = (f32[256]{0:T(256)S(1)}, f32[256]{0:T(256)}, u32[]{:S(2)}) copy-start(f32[256]{0:T(256)} %custom-call) | copy-start | bytes 3076
  266.1 4.0 %copy-start.6 = (bf16[256,2,64]{0,2,1:T(8,128)(2,1)S(1)}, bf16[256,2,64]{0,2,1:T(8,128)(2,1)}, u32[]{:S(2)}) copy-start(bf16[256,2,64]{0,2,1:T(8,128)(2,1)} %pad_maximum_fusion.5) | copy-start | bytes 196612
  266.1 4.0 %copy-start.9 = (f32[2,256]{1,0:T(2,128)S(1)}, f32[2,256]{1,0:T(2,128)}, u32[]{:S(2)}) copy-start(f32[2,256]{1,0:T(2,128)} %broadcast_in_dim.63) | copy-start | bytes 6148
  270.1 21.3 %copy-start.18 = (f32[256]{0:T(256)S(1)}, f32[256]{0:T(256)}, u32[]{:S(2)}) copy-start(f32[256]{0:T(256)} %param.38) | copy-start | bytes 3076
  270.1 21.4 %copy-start.11 = (f32[256]{0:T(256)S(1)}, f32[256]{0:T(256)}, u32[]{:S(2)}) copy-start(f32[256]{0:T(256)} %param.37) | copy-start | bytes 3076
  296.2 30.2 %copy-start.10 = (f32[4096]{0:T(1024)S(1)}, f32[4096]{0:T(1024)}, u32[]{:S(2)}) copy-start(f32[4096]{0:T(1024)} %param.41) | copy-start | bytes 49156
  (5 other events, 9.5 us)
Sparse Core Ops, SparseCore 0:
  8.9 25.2 all-gather.4
  46.3 49.1 all-gather.6
  296.4 28.7 reduce-scatter.1
where the time goes:
time: 339 us; the launch traced here: 335 us
  local copies, waits for them, and re-layouts  107 us (32%)
  blocking collectives  74 us (22%)
  other arithmetic  55.4 us (16%)
  waiting for transfers between devices  52.6 us (16%)
  matrix products  27.6 us (8%)
  between operations  13.5 us (4%)
  starting transfers between devices  4.15 us (1%)
    slice x52, local copies, waits for them, and re-layouts, shards(): lax.associative_scan(combine_steps, (keep_rate, driven), axis=0)  64.7 us
    all_gather x2, blocking collectives, entering(): pieces = jax.tree.map(lambda part: lax.all_gather(part, axis), value)  34.8 us
    all_gather x1, blocking collectives, shards(): rope_source = lax.all_gather(rope_key, 'sp', axis=0, tiled=True)  33.6 us
    reduce_scatter x1, waiting for transfers between devices, shards(): lax.psum_scatter((jnp.dot(rec_norm, w_out_rec, preferred_element_type=jnp...  28.9 us
    pad x28, local copies, waits for them, and re-layouts, shards(): lax.associative_scan(combine_steps, (keep_rate, driven), axis=0)  25.2 us
    all_gather x1, waiting for transfers between devices, shards(): lax.all_gather(tokens, 'tp', axis=1, tiled=True).astype(jnp.float32)  23 us
    add x13, other arithmetic, combine_steps(): return (earlier[0] * later[0], later[0] * earlier[1] + later[1])  17.2 us
    dot_general x5, matrix products, accumulate(): return jnp.dot(source, weight, preferred_element_type=jnp.float32)  14.1 us
  transfers between devices with their start and end apart: 4, of which 2 were waited for; matrix products, arithmetic and copies ran while one was open for 48% of the time, Pallas kernels for 0%

commit v1 on v0

--- a/solution.py
+++ b/solution.py
@@ -1,8 +1,11 @@
+import functools
 import math
 
 import jax
 import jax.numpy as jnp
 from jax import lax
+from jax.experimental import pallas as pl
+from jax.experimental.pallas import tpu as pltpu
 from jax.sharding import PartitionSpec as P
 
 NOPE = 128
@@ -80,6 +83,117 @@
         "hqk,khd->hqd", weights.astype(jnp.bfloat16), values, preferred_element_type=jnp.float32
     )
     return (largest, totals, accumulated)
+
+
+MESH = pl.DeviceIdType.MESH
+
+
+def one_minus_exp(y):
+    series = 1.0 + y * (1.0 / 8.0)
+    for order in (7, 6, 5, 4, 3, 2):
+        series = 1.0 + y * (1.0 / order) * series
+    return jnp.where(y > -0.5, -y * series, 1.0 - jnp.exp(y))
+
+
+def gelu_tanh(x):
+    inner = math.sqrt(2.0 / math.pi) * (x + 0.044715 * (x * x * x))
+    return 0.5 * x * (1.0 + jnp.tanh(inner))
+
+
+def rec_kernel(
+    n, rec_ref, taps_ref, rmap_ref, imap_ref, soft_ref, rate_ref, gate_ref,
+    out_ref, sq_ref, padded, tail_tx, tail_rx, carry_tx, carry_rx, sems, rsems,
+):
+    me = lax.axis_index("sp")
+    rows, channels = rec_ref.shape
+    barrier = pltpu.get_barrier_semaphore()
+    for d in range(1, n):
+        pl.semaphore_signal(
+            barrier, inc=1, device_id={"sp": lax.rem(me + d, n)}, device_id_type=MESH
+        )
+    x = rec_ref[...].astype(jnp.float32)
+    tail_tx[...] = x[rows - 8 :, :]
+    padded[8:, :] = x
+    pl.semaphore_wait(barrier, n - 1)
+    tail = pltpu.make_async_remote_copy(
+        src_ref=tail_tx, dst_ref=tail_rx, send_sem=sems.at[0], recv_sem=rsems.at[0],
+        device_id={"sp": lax.rem(me + 1, n)}, device_id_type=MESH,
+    )
+    tail.start()
+    tail.wait()
+    padded[0:8, :] = jnp.where(me > 0, tail_rx[...], 0.0)
+    count = taps_ref.shape[0]
+    conv = taps_ref[0:1, :] * padded[9 - count : 9 - count + rows, :]
+    for k in range(1, count):
+        conv = conv + taps_ref[k : k + 1, :] * padded[9 - count + k : 9 - count + k + rows, :]
+    low = conv.astype(jnp.bfloat16)
+    width = rmap_ref.shape[1]
+    rate, entry = [], []
+    for b in range(rmap_ref.shape[0]):
+        part = low[:, b * width : (b + 1) * width]
+        rate.append(jnp.dot(part, rmap_ref[b], preferred_element_type=jnp.float32))
+        entry.append(jnp.dot(part, imap_ref[b], preferred_element_type=jnp.float32))
+    rate = jax.nn.sigmoid(jnp.concatenate(rate, axis=1))
+    entry = jax.nn.sigmoid(jnp.concatenate(entry, axis=1))
+    log_keep = -RATE_C * rate_ref[...] * rate * soft_ref[...]
+    a = jnp.exp(log_keep)
+    b = jnp.sqrt(one_minus_exp(2.0 * log_keep)) * entry * conv
+    row = lax.broadcasted_iota(jnp.int32, (rows, channels), 0)
+    d = 1
+    while d < rows:
+        inside = row >= d
+        b = a * jnp.where(inside, pltpu.roll(b, d, 0), 0.0) + b
+        a = a * jnp.where(inside, pltpu.roll(a, d, 0), 1.0)
+        d *= 2
+    carry_tx[...] = jnp.zeros_like(carry_tx)
+    carry_tx[0:1, :] = a[rows - 1 :, :]
+    carry_tx[1:2, :] = b[rows - 1 :, :]
+    copies = []
+    for d in range(1, n):
+        copies.append(
+            pltpu.make_async_remote_copy(
+                src_ref=carry_tx, dst_ref=carry_rx.at[me], send_sem=sems.at[d],
+                recv_sem=rsems.at[d], device_id={"sp": lax.rem(me + d, n)}, device_id_type=MESH,
+            )
+        )
+        copies[-1].start()
+    gated = gelu_tanh(gate_ref[...])
+    for copy in copies:
+        copy.wait()
+    carried = jnp.zeros((1, channels), jnp.float32)
+    for s in range(n - 1):
+        longer = carry_rx[s, 0:1, :] * carried + carry_rx[s, 1:2, :]
+        carried = jnp.where(s < me, longer, carried)
+    rec_out = (b + a * carried) * gated
+    out_ref[...] = rec_out
+    sq_ref[...] = jnp.sum(rec_out * rec_out, axis=1, keepdims=True)
+
+
+def recurrent(rec_input, conv_taps, rate_maps, input_maps, soft, rate, gate_value):
+    n = lax.axis_size("sp")
+    rows, channels = rec_input.shape
+    vmem = pl.BlockSpec(memory_space=pltpu.VMEM)
+    return pl.pallas_call(
+        functools.partial(rec_kernel, n),
+        out_shape=(
+            jax.ShapeDtypeStruct((rows, channels), jnp.float32),
+            jax.ShapeDtypeStruct((rows, 1), jnp.float32),
+        ),
+        in_specs=[vmem] * 7,
+        out_specs=(vmem, vmem),
+        scratch_shapes=[
+            pltpu.VMEM((rows + 8, channels), jnp.float32),
+            pltpu.VMEM((8, channels), jnp.float32),
+            pltpu.VMEM((8, channels), jnp.float32),
+            pltpu.VMEM((8, channels), jnp.float32),
+            pltpu.VMEM((n, 8, channels), jnp.float32),
+            pltpu.SemaphoreType.DMA((n,)),
+            pltpu.SemaphoreType.DMA((n,)),
+        ],
+        compiler_params=pltpu.CompilerParams(collective_id=0, has_side_effects=True),
+        cost_estimate=pl.CostEstimate(flops=20_000_000, bytes_accessed=2_000_000, transcendentals=0),
+        name="recurrent",
+    )(rec_input, conv_taps, rate_maps, input_maps, soft, rate, gate_value)
 
 
 def shards(
@@ -129,34 +243,15 @@
     query_raw = inverse * sum_query
     latent_raw = inverse * sum_latent
     rope_raw = inverse * sum_rope
-    taps = conv_taps.shape[0]
-    tail_rows = rec_input[row_count - (taps - 1) :]
-    before = passed_along(tail_rows, "sp", 1)
-    padded = jnp.concatenate([before, rec_input], axis=0)
-    convolved = conv_taps[0] * padded[0:row_count].astype(jnp.float32)
-    for tap_index in range(1, taps):
-        convolved = convolved + conv_taps[tap_index] * padded[
-            tap_index : tap_index + row_count
-        ].astype(jnp.float32)
-    conv_low = convolved.astype(jnp.bfloat16)
-    blocks = conv_low.reshape(row_count, rate_maps.shape[0], rate_maps.shape[1])
-    rate_gate = jax.nn.sigmoid(
-        jnp.einsum("sbi,bij->sbj", blocks, rate_maps, preferred_element_type=jnp.float32)
-    ).reshape(row_count, channels)
-    entry_gate = jax.nn.sigmoid(
-        jnp.einsum("sbi,bij->sbj", blocks, input_maps, preferred_element_type=jnp.float32)
-    ).reshape(row_count, channels)
-    log_keep = -RATE_C * rate_factor[:, None] * rate_gate * jax.nn.softplus(-decay_param)
-    keep_rate = jnp.exp(log_keep)
-    driven = jnp.sqrt(-jnp.expm1(2.0 * log_keep)) * entry_gate * convolved
-    cum_keep, local_state = lax.associative_scan(combine_steps, (keep_rate, driven), axis=0)
-    identity = (jnp.ones((channels,), jnp.float32), jnp.zeros((channels,), jnp.float32))
-    chain_keep, carried = entering(
-        (cum_keep[row_count - 1], local_state[row_count - 1]), "sp", combine_steps, identity
-    )
-    state_seq = local_state + cum_keep * carried[None, :]
-    rec_out = state_seq * jax.nn.gelu(gate_value)
-    rec_squares = jnp.sum(rec_out * rec_out, axis=1, keepdims=True)
+    rec_out, rec_squares = recurrent(
+        rec_input,
+        conv_taps,
+        rate_maps,
+        input_maps,
+        jax.nn.softplus(-decay_param)[None, :],
+        rate_factor[:, None],
+        gate_value,
+    )
     cosine, sine_part = angles(row_count, first_place, ROPE)
     query_heads = query_raw.reshape(row_count, heads_here, NOPE + ROPE)
     query_nope = query_heads[:, :, :NOPE].astype(jnp.bfloat16)

time: 339 us -> 181 us (0.53)
  local copies, waits for them, and re-layouts: 107 us -> 11.4 us
  other arithmetic: 55.4 us -> 10.6 us
  blocking collectives: 74 us -> 46.8 us
  Pallas kernels: 0 us -> 13.1 us
  waiting for transfers between devices: 52.6 us -> 59.1 us
  starting transfers between devices: 4.15 us -> 0.08 us
    slice x54 -> x0, local copies, waits for them, and re-layouts: 66.7 us -> none  [the longest x52 64.7 us: shards(): lax.associative_scan(combine_steps, (keep_rate, driven), axis=0)]
    all_gather x2 -> x0, blocking collectives: 34.8 us -> none  [entering(): pieces = jax.tree.map(lambda part: lax.all_gather(part, axis), value)]
    add x27 -> x0, other arithmetic: 26.3 us -> none  [the longest x13 17.2 us: combine_steps(): return (earlier[0] * later[0], later[0] * earlier[1] + later[1])]
    pad x28 -> x0, local copies, waits for them, and re-layouts: 25.2 us -> none  [shards(): lax.associative_scan(combine_steps, (keep_rate, driven), axis=0)]
    pallas_call x0 -> x1, Pallas kernels: none -> 13.1 us  [recurrent(): pl.pallas_call(functools.partial(rec_kernel, n), out_shape=(jax.ShapeDtyp...]
    concatenate x14 -> x0, other arithmetic: 11.1 us -> none  [shards(): lax.associative_scan(combine_steps, (keep_rate, driven), axis=0)]
    psum x1, blocking collectives: 5.66 us -> 13.3 us  [shards(): rec_total, att_total = lax.psum((rec_squares, att_squares), 'tp')]
    ppermute x1 -> x0, starting transfers between devices: 4.07 us -> none  [passed_along(): return lax.ppermute(block, axis, route)]
  transfers between devices with their start and end apart: 4 -> 3, of which waited for: 2 -> 2; matrix products, arithmetic and copies ran while one was open for 48% -> 9% of each run, Pallas kernels for 0% -> 7%
where the time goes in v1:
time: 181 us; the launch traced here: 180 us
  waiting for transfers between devices  59.1 us (33%)
  blocking collectives  46.8 us (26%)
  matrix products  25.6 us (14%)
  between operations  13.3 us (7%)
  Pallas kernels  13.1 us (7%)
  local copies, waits for them, and re-layouts  11.4 us (6%)
  other arithmetic  10.6 us (6%)
    all_gather x1, blocking collectives, shards(): rope_source = lax.all_gather(rope_key, 'sp', axis=0, tiled=True)  33.6 us
    reduce_scatter x1, waiting for transfers between devices, shards(): lax.psum_scatter((jnp.dot(rec_norm, w_out_rec, preferred_element_type=jnp...  31.4 us
    all_gather x1, waiting for transfers between devices, shards(): lax.all_gather(tokens, 'tp', axis=1, tiled=True).astype(jnp.float32)  26.9 us
    dot_general x5, matrix products, accumulate(): return jnp.dot(source, weight, preferred_element_type=jnp.float32)  14.9 us
    psum x1, blocking collectives, shards(): rec_total, att_total = lax.psum((rec_squares, att_squares), 'tp')  13.3 us
    pallas_call x1, Pallas kernels, recurrent(): pl.pallas_call(functools.partial(rec_kernel, n), out_shape=(jax.ShapeDtyp...  13.1 us
    another operation x2, local copies, waits for them, and re-layouts  5.8 us
  transfers between devices with their start and end apart: 3, of which 2 were waited for; matrix products, arithmetic and copies ran while one was open for 9% of the time, Pallas kernels for 7%

profile of v1, /device:TPU:0, one launch (start us, length us, event | category | flops | bytes accessed | tf_op | source)
XLA Modules:
  0.0 180.0 jit_solution(3048201556429894492)
XLA Ops:
  7.3 26.9 %all-gather.3.cloned.1.call-done = bf16[256,4096]{1,0:T(8,128)(2,1)} async-done(((bf16[256,1024]{1,0:T(8,128)(2,1)}), bf16[256,4096]{1,0:T(8,128)(2,1)}) %all-gather.3.cloned.1.call-update) | async-done | bytes 2097168 | tf_op jit(solution)/shard_map/all_gather | solution.py:228
  34.2 2.2 %fusion.15 = f32[256]{0:T(256)S(1)} fusion(bf16[256,4096]{1,0:T(8,128)(2,1)} %all-gather.3.cloned.1.call-done), kind=kLoop, calls=%fused_computation.23 | loop fusion | flops 3145472 | bytes 2098176 | tf_op jit(solution)/shard_map/reduce_sum | solution.py:234
  36.5 3.6 %multiply_reduce_fusion = (f32[256]{0:T(256)S(1)}, f32[256,512]{1,0:T(8,128)S(1)}) fusion(bf16[4096,512]{1,0:T(8,128)(2,1)} %param.31, bf16[256,4096]{1,0:T(8,128)(2,1)S(1)} %copy-done.2, f32[4096]{0:T(1024)S(1)} %copy-done.14, f32[256]{0:T(256)S(1)} %add_rsqrt_fusion.1), kind=kOutput, calls=%fused_computation.38 | convolution fusion | flops 1077280512 | bytes 6834176 | tf_op jit(solution)/shard_map/dot_general | solution.py:232
  42.7 3.6 %convolution_multiply_fusion.1 = f32[256,384]{1,0:T(8,128)} fusion(bf16[4096,384]{1,0:T(8,128)(2,1)S(1)} %copy-done, bf16[256,4096]{1,0:T(8,128)(2,1)} %all-gather.3.cloned.1.call-done, f32[4096]{0:T(1024)S(1)} %copy-done.14, f32[256]{0:T(256)S(1)} %add_rsqrt_fusion.1), kind=kOutput, calls=%fused_computation.29 | convolution fusion | flops 808550400 | bytes 5653504 | tf_op jit(solution)/shard_map/dot_general | solution.py:232
  46.3 1.9 %copy.28 = f32[256,384]{0,1:T(8,128)} copy(f32[256,384]{1,0:T(8,128)} %convolution_multiply_fusion.1) | data formatting | bytes 786432 | tf_op jit(solution)/shard_map/mul | solution.py:243
  48.3 3.9 %convolution_multiply_fusion.2.gate_ref = f32[256,256]{1,0:T(8,128)} fusion(bf16[4096,256]{1,0:T(8,128)(2,1)} %param.25, bf16[256,4096]{1,0:T(8,128)(2,1)} %all-gather.3.cloned.1.call-done, f32[4096]{0:T(1024)S(1)} %copy-done.14, f32[256]{0:T(256)S(1)} %add_rsqrt_fusion.1), kind=kOutput, calls=%fused_computation.30 | convolution fusion | flops 540082176 | bytes 4473856 | tf_op jit(solution)/shard_map/dot_general | solution.py:232
  52.2 1.4 fusion.17.rec_ref
  53.6 13.1 %recurrent.1 = (f32[256,256]{1,0:T(8,128)}, f32[256,1]{1,0:T(8,128)}) custom-call(bf16[256,256]{1,0:T(8,128)(2,1)} %fusion.17.rec_ref, f32[4,256]{1,0:T(4,128)} %taps_ref.1, bf16[2,128,128]{2,1,0:T(8,128)(2,1)} %rmap_ref.1, bf16[2,128,128]{2,1,0:T(8,128)(2,1)} %imap_ref.1, f32[1,256]{1,0:T(1,128)} %bitcast.42, f32[256,1]{1,0:T(8,128)} %copy.27.rate_ref, ...), custom_call_target="tpu_custom_call" | custom-call | flops 20000000 | bytes 2000000 | tf_op jit(solution)/shard_map/recurrent/pallas_call | solution.py:176
  66.6 2.4 %convolution_multiply_fusion.4 = f32[256,64]{0,1:T(8,128)S(1)} fusion(bf16[4096,64]{0,1:T(8,128)(2,1)} %param.32, bf16[256,4096]{1,0:T(8,128)(2,1)} %all-gather.3.cloned.1.call-done, f32[4096]{0:T(1024)S(1)} %copy-done.14, f32[256]{0:T(256)S(1)} %add_rsqrt_fusion.1), kind=kOutput, calls=%fused_computation.33 | convolution fusion | flops 137379840 | bytes 2704384 | tf_op jit(solution)/shard_map/dot_general | solution.py:232
  70.2 33.6 %all_gather.11 = bf16[2048,64]{0,1:T(8,128)(2,1)} all-gather(bf16[256,64]{0,1:T(8,128)(2,1)S(1)} %pad_maximum_fusion.1), channel_id=1, replica_groups=mesh['sp'=8,'tp'=4] {'sp'}, dimensions={0}, use_global_device_ids=true | all-gather | bytes 294912 | tf_op jit(solution)/shard_map/all_gather | solution.py:272
  103.8 14.5 %conditional.1 = (f32[2,256]{1,0:T(2,128)S(1)}, f32[2,256,128]{1,2,0:T(8,128)}) conditional(s32[]{:T(128)} %convert_element_type.61, (f32[2,256]{1,0:T(2,128)S(1)}, f32[2,256,128]{2,1,0:T(8,128)S(1)}) %tuple.25, (s32[]{:T(128)}, s32[256]{0:T(256)S(1)}, bf16[2048,512]{1,0:T(8,128)(2,1)}, f32[256,2,192]{0,2,1:T(8,128)}, bf16[2048,64]{0,1:T(8,128)(2,1)}, ...), branch_computations={%region_3.0_spmd, %region_4.7_spmd} | conditional | flops 680135424 | bytes 39873612 | solution.py:298
  103.8 4.0 %copy.29 = bf16[2048,512]{0,1:T(8,128)(2,1)} copy(bf16[2048,512]{1,0:T(8,128)(2,1)} %get-tuple-element.148) | data formatting | bytes 4194304 | tf_op jit(solution)/shard_map
  107.8 1.8 %copy.30 = bf16[256,2,192]{2,0,1:T(8,128)(2,1)} copy(f32[256,2,192]{0,2,1:T(8,128)} %get-tuple-element.149) | data formatting | bytes 589824 | tf_op jit(solution)/shard_map
  109.6 2.0 %fusion.11 = f32[2,256,2048]{2,1,0:T(8,128)S(1)} fusion(bf16[2048,2,256]{0,2,1:T(8,128)(2,1)} %bitcast.37, bf16[256,2,192]{2,0,1:T(8,128)(2,1)} %copy.30), kind=kOutput, calls=%fused_computation.11 | convolution fusion | flops 268435456 | bytes 5373952 | tf_op jit(solution)/shard_map/while/body/eval_jaxpr/cond/branch_1_fun/qhd,khd->hqk/dot_general | solution.py:69
  112.0 1.3 fusion.34
  115.0 1.6 fusion.7
  116.6 1.8 copy.35
  119.5 13.3 %all-reduce = (f32[256,1]{1,0:T(8,128)}, f32[256,1]{1,0:T(8,128)}) all-reduce(f32[256,1]{1,0:T(8,128)} %get-tuple-element.133, f32[256,1]{1,0:T(8,128)S(1)} %copy.32), channel_id=1, replica_groups=mesh['sp'=8,'tp'=4] {'tp'}, use_global_device_ids=true, to_apply=%region_1.2 | all-reduce | flops 512 | bytes 4096 | tf_op jit(solution)/shard_map/psum | solution.py:305
  132.8 1.1 rsqrt_reduce_fusion
  134.0 2.6 %fusion.31 = f32[256,4096]{1,0:T(8,128)S(1)} fusion(bf16[256,4096]{1,0:T(8,128)(2,1)} %param.37, f32[256,256]{1,0:T(8,128)} %get-tuple-element.132, f32[256]{0:T(256)S(1)} %copy-done.8, f32[256]{0:T(256)S(1)} %get-tuple-element.176), kind=kOutput, calls=%fused_computation.47 | convolution fusion | flops 537067520 | bytes 6555648 | tf_op jit(solution)/shard_map/dot_general | solution.py:314
  136.6 2.1 %fusion.14 = bf16[256,4096]{1,0:T(8,128)(2,1)} fusion(f32[256,4096]{1,0:T(8,128)S(1)} %fusion.31, bf16[256,256]{0,1:T(8,128)(2,1)S(1)} %fusion.27, bf16[256,4096]{1,0:T(8,128)(2,1)S(1)} %copy-done.4), kind=kOutput, calls=%fused_computation.22 | convolution fusion | flops 538968064 | bytes 8519680 | tf_op jit(solution)/shard_map/dot_general | solution.py:315
  138.7 31.4 %reduce-scatter.2.cloned.1.call-done = bf16[64,4096]{1,0:T(8,128)(2,1)} async-done(((bf16[256,4096]{1,0:T(8,128)(2,1)}), bf16[64,4096]{1,0:T(8,128)(2,1)}) %reduce-scatter.2.cloned.1.call-update) | async-done | bytes 524304 | tf_op jit(solution)/shard_map/reduce_scatter | solution.py:312
  170.2 1.2 fusion.23
  171.4 2.0 %fusion.25 = bf16[64,4096]{1,0:T(8,128)(2,1)} fusion(bf16[64,4096]{1,0:T(8,128)(2,1)} %reduce-scatter.2.cloned.1.call-done, f32[4096]{0:T(1024)S(1)} %copy-done.7, f32[64]{0:T(128)S(1)} %add_rsqrt_fusion.2), kind=kLoop, calls=%fused_computation.36 | loop fusion | flops 1048576 | bytes 1065216 | tf_op jit(solution)/shard_map/convert_element_type | solution.py:321
  (60 shorter events, 7.7 us)
Async XLA Ops:
  6.5 36.2 %copy-start = (bf16[4096,384]{1,0:T(8,128)(2,1)S(1)}, bf16[4096,384]{1,0:T(8,128)(2,1)}, u32[]{:S(2)}) copy-start(bf16[4096,384]{1,0:T(8,128)(2,1)} %param.30) | copy-start | bytes 9437188
  6.5 29.9 %copy-start.14 = (f32[4096]{0:T(1024)S(1)}, f32[4096]{0:T(1024)}, u32[]{:S(2)}) copy-start(f32[4096]{0:T(1024)} %param.22) | copy-start | bytes 49156
  6.5 27.7 %all-gather.3.cloned.1.call-start = ((), (), s32[]{:S(2)}) async-start(), calls=%async_computation.1 | async-start | bytes 2621440 | tf_op jit(solution)/shard_map/all_gather | solution.py:228
  7.3 96.5 %all-gather.5.cloned.1.call-start = ((), (), s32[]{:S(2)}) async-start(), calls=%async_computation.2 | async-start | bytes 2359296 | tf_op jit(solution)/shard_map/all_gather | solution.py:271
  34.2 2.3 %copy-start.2 = (bf16[256,4096]{1,0:T(8,128)(2,1)S(1)}, bf16[256,4096]{1,0:T(8,128)(2,1)}, u32[]{:S(2)}) copy-start(bf16[256,4096]{1,0:T(8,128)(2,1)} %all-gather.3.cloned.1.call-done) | copy-start | bytes 6291460
  36.5 3.6 %copy-start.6 = (bf16[512,512]{1,0:T(8,128)(2,1)S(1)}, bf16[512,512]{1,0:T(8,128)(2,1)}, u32[]{:S(2)}) copy-start(bf16[512,512]{1,0:T(8,128)(2,1)} %param.34) | copy-start | bytes 1572868
  36.5 3.6 %copy-start.9 = (f32[512]{0:T(512)S(1)}, f32[512]{0:T(512)}, u32[]{:S(2)}) copy-start(f32[512]{0:T(512)} %param.33) | copy-start | bytes 6148
  36.5 4.8 %copy-start.10 = (f32[256]{0:T(256)S(1)}, f32[256]{0:T(256)}, u32[]{:S(2)}) copy-start(f32[256]{0:T(256)} %param.23) | copy-start | bytes 3076
  36.5 5.6 %copy-start.12 = (f32[256]{0:T(256)S(1)}, f32[256]{0:T(256)}, u32[]{:S(2)}) copy-start(f32[256]{0:T(256)} %param.29) | copy-start | bytes 3076
  41.2 128.9 %reduce-scatter.2.cloned.1.call-start = ((), (), s32[]{:S(2)}) async-start(), calls=%async_computation.3 | async-start | bytes 2621440 | tf_op jit(solution)/shard_map/reduce_scatter | solution.py:312
  48.2 4.0 %copy-start.3 = (bf16[256,4096]{1,0:T(8,128)(2,1)S(1)}, bf16[256,4096]{1,0:T(8,128)(2,1)}, u32[]{:S(2)}) copy-start(bf16[256,4096]{1,0:T(8,128)(2,1)} %all-gather.3.cloned.1.call-done) | copy-start | bytes 6291460
  48.2 4.0 %copy-start.13 = (bf16[4096,256]{1,0:T(8,128)(2,1)S(1)}, bf16[4096,256]{1,0:T(8,128)(2,1)}, u32[]{:S(2)}) copy-start(bf16[4096,256]{1,0:T(8,128)(2,1)} %param.24) | copy-start | bytes 6291460
  103.8 30.1 %copy-start.11 = (f32[256]{0:T(256)S(1)}, f32[256]{0:T(256)}, u32[]{:S(2)}) copy-start(f32[256]{0:T(256)} %param.36) | copy-start | bytes 3076
  103.8 30.2 %copy-start.8 = (f32[256]{0:T(256)S(1)}, f32[256]{0:T(256)}, u32[]{:S(2)}) copy-start(f32[256]{0:T(256)} %param.35) | copy-start | bytes 3076
  109.6 2.4 %copy-start.5 = (bf16[2048,64]{0,1:T(8,128)(2,1)S(1)}, bf16[2048,64]{0,1:T(8,128)(2,1)}, u32[]{:S(2)}) copy-start(bf16[2048,64]{0,1:T(8,128)(2,1)} %get-tuple-element.125) | copy-start | bytes 786436 | tf_op jit(solution)/shard_map/while/body/eval_jaxpr/cond
  113.4 1.6 copy-start.1
  134.0 2.6 %copy-start.4 = (bf16[256,4096]{1,0:T(8,128)(2,1)S(1)}, bf16[256,4096]{1,0:T(8,128)(2,1)}, u32[]{:S(2)}) copy-start(bf16[256,4096]{1,0:T(8,128)(2,1)} %param.38) | copy-start | bytes 6291460
  138.7 32.7 %copy-start.7 = (f32[4096]{0:T(1024)S(1)}, f32[4096]{0:T(1024)}, u32[]{:S(2)}) copy-start(f32[4096]{0:T(1024)} %param.39) | copy-start | bytes 49156
Sparse Core Ops, SparseCore 0:
  8.9 25.2 all-gather.2
  41.3 52.4 all-gather.4
  138.8 31.2 reduce-scatter.1

commit v2 on v1

--- a/solution.py
+++ b/solution.py
@@ -102,7 +102,7 @@
 
 def rec_kernel(
     n, rec_ref, taps_ref, rmap_ref, imap_ref, soft_ref, rate_ref, gate_ref,
-    out_ref, sq_ref, padded, tail_tx, tail_rx, carry_tx, carry_rx, sems, rsems,
+    out_ref, padded, tail_tx, tail_rx, carry_tx, carry_rx, sems, rsems,
 ):
     me = lax.axis_index("sp")
     rows, channels = rec_ref.shape
@@ -166,7 +166,6 @@
         carried = jnp.where(s < me, longer, carried)
     rec_out = (b + a * carried) * gated
     out_ref[...] = rec_out
-    sq_ref[...] = jnp.sum(rec_out * rec_out, axis=1, keepdims=True)
 
 
 def recurrent(rec_input, conv_taps, rate_maps, input_maps, soft, rate, gate_value):
@@ -175,12 +174,9 @@
     vmem = pl.BlockSpec(memory_space=pltpu.VMEM)
     return pl.pallas_call(
         functools.partial(rec_kernel, n),
-        out_shape=(
-            jax.ShapeDtypeStruct((rows, channels), jnp.float32),
-            jax.ShapeDtypeStruct((rows, 1), jnp.float32),
-        ),
+        out_shape=jax.ShapeDtypeStruct((rows, channels), jnp.float32),
         in_specs=[vmem] * 7,
-        out_specs=(vmem, vmem),
+        out_specs=vmem,
         scratch_shapes=[
             pltpu.VMEM((rows + 8, channels), jnp.float32),
             pltpu.VMEM((8, channels), jnp.float32),
@@ -194,6 +190,143 @@
         cost_estimate=pl.CostEstimate(flops=20_000_000, bytes_accessed=2_000_000, transcendentals=0),
         name="recurrent",
     )(rec_input, conv_taps, rate_maps, input_maps, soft, rate, gate_value)
+
+
+def out_kernel(
+    n, rec_ref, att_ref, rgain_ref, again_ref, wrec_ref, watt_ref, post_ref, out_ref,
+    rec_norm, att_norm, sq_tx, sq_rx, part, rx1, tx2, rx2, mixed,
+    sq_s, sq_r, s1, r1, s2, r2,
+):
+    me = lax.axis_index("tp")
+    core, group = lax.rem(me, 2), me // 2
+    groups = n // 2
+    rows = rec_ref.shape[0]
+    chunks, _, _, block, cols = part.shape
+    barrier = pltpu.get_barrier_semaphore()
+    for d in range(1, n):
+        pl.semaphore_signal(
+            barrier, inc=1, device_id={"tp": lax.rem(me + d, n)}, device_id_type=MESH
+        )
+
+    def row_squares(ref):
+        x = ref[...]
+        ones = jnp.ones((8, x.shape[1]), jnp.float32)
+        return lax.dot_general(
+            ones, x * x, (((1,), (1,)), ((), ())),
+            precision=lax.Precision.HIGHEST, preferred_element_type=jnp.float32,
+        )
+
+    which = lax.broadcasted_iota(jnp.int32, (8, rows), 0)
+    sq_tx[...] = jnp.where(which < 4, row_squares(rec_ref), row_squares(att_ref))
+    pl.semaphore_wait(barrier, n - 1)
+    copies = []
+    for d in range(1, n):
+        copies.append(
+            pltpu.make_async_remote_copy(
+                src_ref=sq_tx, dst_ref=sq_rx.at[d - 1], send_sem=sq_s.at[d - 1],
+                recv_sem=sq_r.at[d - 1], device_id={"tp": lax.rem(me + d, n)},
+                device_id_type=MESH,
+            )
+        )
+        copies[-1].start()
+    total = sq_tx[...]
+    for d in range(1, n):
+        copies[d - 1].wait()
+        total = total + sq_rx[d - 1]
+    total = jnp.transpose(total)
+    rec_inv = lax.rsqrt(total[:, 0:1] / (rec_ref.shape[1] * n) + EPS)
+    att_inv = lax.rsqrt(total[:, 4:5] / (att_ref.shape[1] * n) + EPS)
+    rec_norm[...] = (rec_ref[...] * rec_inv * rgain_ref[...]).astype(jnp.bfloat16)
+    att_norm[...] = (att_ref[...] * att_inv * again_ref[...]).astype(jnp.bfloat16)
+    partner = group * 2 + (1 - core)
+    first, second = [], []
+
+    def cross(k):
+        first[k].wait()
+        pair = part[k, core].astype(jnp.float32) + rx1[k].astype(jnp.float32)
+        tx2[k] = pair.astype(jnp.bfloat16)
+        for e in range(1, groups):
+            other = lax.rem(group + e, groups)
+            second.append(
+                pltpu.make_async_remote_copy(
+                    src_ref=tx2.at[k, other], dst_ref=rx2.at[k, e - 1],
+                    send_sem=s2.at[k, e - 1], recv_sem=r2.at[k, e - 1],
+                    device_id={"tp": other * 2 + core}, device_id_type=MESH,
+                )
+            )
+            second[-1].start()
+
+    step = min(cols, 256)
+    for k in range(chunks):
+        for at in range(0, cols, step):
+            here = slice(k * cols + at, k * cols + at + step)
+            piece = (
+                jnp.dot(rec_norm[...], wrec_ref[:, here], preferred_element_type=jnp.float32)
+                + jnp.dot(att_norm[...], watt_ref[:, here], preferred_element_type=jnp.float32)
+            ).astype(jnp.bfloat16)
+            for j in range(n):
+                part[k, j % 2, j // 2, :, at : at + step] = piece[j * block : (j + 1) * block]
+        first.append(
+            pltpu.make_async_remote_copy(
+                src_ref=part.at[k, 1 - core], dst_ref=rx1.at[k], send_sem=s1.at[k],
+                recv_sem=r1.at[k], device_id={"tp": partner}, device_id_type=MESH,
+            )
+        )
+        first[-1].start()
+        if k > 0:
+            cross(k - 1)
+    cross(chunks - 1)
+    squares = jnp.zeros((block, 1), jnp.float32)
+    for k in range(chunks):
+        value = tx2[k, group].astype(jnp.float32)
+        for e in range(1, groups):
+            second[k * (groups - 1) + e - 1].wait()
+            value = value + rx2[k, e - 1].astype(jnp.float32)
+        mixed[k] = value
+        squares = squares + jnp.sum(value * value, axis=1, keepdims=True)
+    inverse = lax.rsqrt(squares / (chunks * cols) + EPS)
+    for k in range(chunks):
+        here = slice(k * cols, (k + 1) * cols)
+        out_ref[:, here] = (mixed[k] * inverse * post_ref[:, here]).astype(jnp.bfloat16)
+
+
+def project_out(rec_out, att_out, rec_gain, att_gain, w_out_rec, w_out_att, post_gain):
+    n = lax.axis_size("tp")
+    rows, channels = rec_out.shape
+    width = w_out_rec.shape[1]
+    chunks = math.gcd(width // 128, 4)
+    cols, block, groups = width // chunks, rows // n, n // 2
+    vmem = pl.BlockSpec(memory_space=pltpu.VMEM)
+    low, dma = jnp.bfloat16, pltpu.SemaphoreType.DMA
+    far = max(groups - 1, 1)
+    return pl.pallas_call(
+        functools.partial(out_kernel, n),
+        out_shape=jax.ShapeDtypeStruct((block, width), low),
+        in_specs=[vmem] * 7,
+        out_specs=vmem,
+        scratch_shapes=[
+            pltpu.VMEM((rows, channels), low),
+            pltpu.VMEM(att_out.shape, low),
+            pltpu.VMEM((8, rows), jnp.float32),
+            pltpu.VMEM((n - 1, 8, rows), jnp.float32),
+            pltpu.VMEM((chunks, 2, groups, block, cols), low),
+            pltpu.VMEM((chunks, groups, block, cols), low),
+            pltpu.VMEM((chunks, groups, block, cols), low),
+            pltpu.VMEM((chunks, far, block, cols), low),
+            pltpu.VMEM((chunks, block, cols), jnp.float32),
+            dma((n - 1,)),
+            dma((n - 1,)),
+            dma((chunks,)),
+            dma((chunks,)),
+            dma((chunks, far)),
+            dma((chunks, far)),
+        ],
+        compiler_params=pltpu.CompilerParams(collective_id=1, has_side_effects=True),
+        cost_estimate=pl.CostEstimate(
+            flops=4 * rows * channels * width, bytes_accessed=8_000_000, transcendentals=0
+        ),
+        name="project_out",
+    )(rec_out, att_out, rec_gain[None, :], att_gain[None, :], w_out_rec, w_out_att, post_gain[None, :])
 
 
 def shards(
@@ -219,9 +352,7 @@
 ):
     row_count = tokens.shape[0]
     model_width = w_rec_in.shape[0]
-    channels = w_rec_in.shape[1]
     heads_here = w_query.shape[1] // (NOPE + ROPE)
-    group_size = lax.axis_size("tp")
     first_place = lax.axis_index("sp") * row_count
     places = first_place + jnp.arange(row_count)
     last_place = first_place + row_count - 1
@@ -243,7 +374,7 @@
     query_raw = inverse * sum_query
     latent_raw = inverse * sum_latent
     rope_raw = inverse * sum_rope
-    rec_out, rec_squares = recurrent(
+    rec_out = recurrent(
         rec_input,
         conv_taps,
         rate_maps,
@@ -301,24 +432,7 @@
     att_out = (
         (accumulated / totals[..., None]).transpose(1, 0, 2).reshape(row_count, heads_here * VDIM)
     )
-    att_squares = jnp.sum(att_out * att_out, axis=1, keepdims=True)
-    rec_total, att_total = lax.psum((rec_squares, att_squares), "tp")
-    rec_norm = (rec_out * lax.rsqrt(rec_total / (channels * group_size) + EPS) * rec_gain).astype(
-        jnp.bfloat16
-    )
-    att_norm = (
-        att_out * lax.rsqrt(att_total / (heads_here * VDIM * group_size) + EPS) * att_gain
-    ).astype(jnp.bfloat16)
-    mixed_sum = lax.psum_scatter(
-        (
-            jnp.dot(rec_norm, w_out_rec, preferred_element_type=jnp.float32)
-            + jnp.dot(att_norm, w_out_att, preferred_element_type=jnp.float32)
-        ).astype(jnp.bfloat16),
-        "tp",
-        scatter_dimension=0,
-        tiled=True,
-    ).astype(jnp.float32)
-    return (mixed_sum * rms_inverse(mixed_sum) * post_gain).astype(jnp.bfloat16)
+    return project_out(rec_out, att_out, rec_gain, att_gain, w_out_rec, w_out_att, post_gain)
 
 
 def solution(mesh):

time: 181 us -> 149 us (0.82)
  waiting for transfers between devices: 59.1 us -> 27.6 us
  Pallas kernels: 13.1 us -> 35.3 us
  blocking collectives: 46.8 us -> 33.8 us
  other arithmetic: 10.6 us -> 5.78 us
  matrix products: 25.6 us -> 20.9 us
    reduce_scatter x1 -> x0, waiting for transfers between devices: 31.4 us -> none  [shards(): lax.psum_scatter((jnp.dot(rec_norm, w_out_rec, preferred_element_type=jnp...]
    pallas_call x1 -> x2, Pallas kernels: 13.1 us -> 35.3 us  [the longest x1 22.4 us: project_out(): pl.pallas_call(functools.partial(out_kernel, n), out_shape=jax.ShapeDtype...]
    psum x1 -> x0, blocking collectives: 13.3 us -> none  [shards(): rec_total, att_total = lax.psum((rec_squares, att_squares), 'tp')]
    dot_general x2 -> x0, matrix products: 4.66 us -> none  [the longest x1 2.57 us: shards(): jnp.dot(rec_norm, w_out_rec, preferred_element_type=jnp.float32)]
    reduce_sum x2 -> x0, other arithmetic: 2.26 us -> none  [the longest x1 1.24 us: rms_inverse(): return lax.rsqrt(jnp.mean(values * values, axis=-1, keepdims=True) + EPS)]
    convert_element_type x2 -> x0, other arithmetic: 2.13 us -> none  [the longest x1 2.02 us: shards(): return (mixed_sum * rms_inverse(mixed_sum) * post_gain).astype(jnp.bfloat16)]
    unnamed x26 -> x17, local copies, waits for them, and re-layouts: 0.06 us -> 1.91 us
  transfers between devices with their start and end apart: 3 -> 2, of which waited for: 2 -> 1; matrix products, arithmetic and copies ran while one was open for 9% -> 11% of each run, Pallas kernels for 7% -> 9%
where the time goes in v2:
time: 149 us; the launch traced here: 148 us
  Pallas kernels  35.3 us (24%)
  blocking collectives  33.8 us (23%)
  waiting for transfers between devices  27.6 us (19%)
  matrix products  20.9 us (14%)
  between operations  13.5 us (9%)
  local copies, waits for them, and re-layouts  11.3 us (8%)
  other arithmetic  5.78 us (4%)
    all_gather x1, blocking collectives, shards(): rope_source = lax.all_gather(rope_key, 'sp', axis=0, tiled=True)  33.8 us
    all_gather x1, waiting for transfers between devices, shards(): lax.all_gather(tokens, 'tp', axis=1, tiled=True).astype(jnp.float32)  26.9 us
    pallas_call x1, Pallas kernels, project_out(): pl.pallas_call(functools.partial(out_kernel, n), out_shape=jax.ShapeDtype...  22.4 us
    dot_general x5, matrix products, accumulate(): return jnp.dot(source, weight, preferred_element_type=jnp.float32)  15.6 us
    pallas_call x1, Pallas kernels, recurrent(): pl.pallas_call(functools.partial(rec_kernel, n), out_shape=jax.ShapeDtype...  12.9 us
    another operation x2, local copies, waits for them, and re-layouts  5.81 us
  transfers between devices with their start and end apart: 2, of which 1 were waited for; matrix products, arithmetic and copies ran while one was open for 11% of the time, Pallas kernels for 9%

profile of v2, /device:TPU:0, one launch (start us, length us, event | category | flops | bytes accessed | tf_op | source)
XLA Modules:
  0.0 148.4 jit_solution(8776375579382019745)
XLA Ops:
  6.5 0.7 all-gather.3.cloned.1.call-update
  7.3 26.9 %all-gather.3.cloned.1.call-done = bf16[256,4096]{1,0:T(8,128)(2,1)} async-done(((bf16[256,1024]{1,0:T(8,128)(2,1)}), bf16[256,4096]{1,0:T(8,128)(2,1)}) %all-gather.3.cloned.1.call-update) | async-done | bytes 2097168 | tf_op jit(solution)/shard_map/all_gather | solution.py:359
  34.2 2.1 %fusion.14 = f32[256]{0:T(256)S(1)} fusion(bf16[256,4096]{1,0:T(8,128)(2,1)} %all-gather.3.cloned.1.call-done), kind=kLoop, calls=%fused_computation.21 | loop fusion | flops 3145472 | bytes 2098176 | tf_op jit(solution)/shard_map/reduce_sum | solution.py:365
  36.4 4.2 %multiply_reduce_fusion = (f32[256]{0:T(256)S(1)}, f32[256,512]{1,0:T(8,128)S(1)}) fusion(bf16[4096,512]{1,0:T(8,128)(2,1)} %param.31, bf16[256,4096]{1,0:T(8,128)(2,1)} %all-gather.3.cloned.1.call-done, f32[4096]{0:T(1024)} %param.22, f32[256]{0:T(256)S(1)} %add_rsqrt_fusion.1), kind=kOutput, calls=%fused_computation.31 | convolution fusion | flops 1077280512 | bytes 6834176 | tf_op jit(solution)/shard_map/dot_general | solution.py:363
  40.6 1.1 convolution_convert_fusion
  41.7 0.8 copy.28.rate_ref
  43.2 3.6 %convolution_multiply_fusion.1 = f32[256,384]{1,0:T(8,128)} fusion(bf16[4096,384]{1,0:T(8,128)(2,1)S(1)} %copy-done, bf16[256,4096]{1,0:T(8,128)(2,1)} %all-gather.3.cloned.1.call-done, f32[4096]{0:T(1024)S(1)} %copy-done.9, f32[256]{0:T(256)S(1)} %add_rsqrt_fusion.1), kind=kOutput, calls=%fused_computation.25 | convolution fusion | flops 808550400 | bytes 5653504 | tf_op jit(solution)/shard_map/dot_general | solution.py:363
  46.8 1.9 %copy.29 = f32[256,384]{0,1:T(8,128)} copy(f32[256,384]{1,0:T(8,128)} %convolution_multiply_fusion.1) | data formatting | bytes 786432 | tf_op jit(solution)/shard_map/mul | solution.py:374
  48.8 3.9 %convolution_multiply_fusion.2.gate_ref = f32[256,256]{1,0:T(8,128)} fusion(bf16[4096,256]{1,0:T(8,128)(2,1)} %param.25, bf16[256,4096]{1,0:T(8,128)(2,1)} %all-gather.3.cloned.1.call-done, f32[4096]{0:T(1024)S(1)} %copy-done.9, f32[256]{0:T(256)S(1)} %add_rsqrt_fusion.1), kind=kOutput, calls=%fused_computation.26 | convolution fusion | flops 540082176 | bytes 4473856 | tf_op jit(solution)/shard_map/dot_general | solution.py:363
  52.7 1.4 fusion.16.rec_ref
  54.1 12.9 %recurrent.1.rec_ref = f32[256,256]{1,0:T(8,128)} custom-call(bf16[256,256]{1,0:T(8,128)(2,1)} %fusion.16.rec_ref, f32[4,256]{1,0:T(4,128)} %taps_ref.1, bf16[2,128,128]{2,1,0:T(8,128)(2,1)} %rmap_ref.1, bf16[2,128,128]{2,1,0:T(8,128)(2,1)} %imap_ref.1, f32[1,256]{1,0:T(1,128)} %bitcast.36, f32[256,1]{1,0:T(8,128)} %copy.28.rate_ref, ...), custom_call_target="tpu_custom_call" | custom-call | flops 20000000 | bytes 2000000 | tf_op jit(solution)/shard_map/recurrent/pallas_call | solution.py:175
  67.0 2.4 %convolution_multiply_fusion.4 = f32[256,64]{0,1:T(8,128)S(1)} fusion(bf16[4096,64]{0,1:T(8,128)(2,1)} %param.32, bf16[256,4096]{1,0:T(8,128)(2,1)} %all-gather.3.cloned.1.call-done, f32[4096]{0:T(1024)S(1)} %copy-done.9, f32[256]{0:T(256)S(1)} %add_rsqrt_fusion.1), kind=kOutput, calls=%fused_computation.29 | convolution fusion | flops 137379840 | bytes 2704384 | tf_op jit(solution)/shard_map/dot_general | solution.py:363
  69.7 0.9 subtract_convert_fusion
  70.6 33.8 %all_gather.11 = bf16[2048,64]{0,1:T(8,128)(2,1)} all-gather(bf16[256,64]{0,1:T(8,128)(2,1)S(1)} %pad_maximum_fusion.1), channel_id=1, replica_groups=mesh['sp'=8,'tp'=4] {'sp'}, dimensions={0}, use_global_device_ids=true | all-gather | bytes 294912 | tf_op jit(solution)/shard_map/all_gather | solution.py:403
  104.4 12.1 %conditional.1 = ((f32[2,256]{1,0:T(2,128)S(1)}, f32[2,256,128]{2,1,0:T(8,128)S(1)})) conditional(s32[]{:T(128)} %convert_element_type.45, (f32[2,256]{1,0:T(2,128)S(1)}, f32[2,256,128]{2,1,0:T(8,128)S(1)}) %tuple.25, (s32[]{:T(128)}, s32[256]{0:T(256)S(1)}, bf16[2048,512]{1,0:T(8,128)(2,1)}, f32[256,2,192]{0,2,1:T(8,128)}, ...), branch_computations={%region_2.3_spmd, %region_3.6_spmd} | conditional | flops 680135424 | bytes 39349332 | solution.py:429
  104.4 4.0 %copy.30 = bf16[2048,512]{0,1:T(8,128)(2,1)} copy(bf16[2048,512]{1,0:T(8,128)(2,1)} %get-tuple-element.144) | data formatting | bytes 4194304 | tf_op jit(solution)/shard_map
  108.3 1.8 %copy.31 = bf16[256,2,192]{2,0,1:T(8,128)(2,1)} copy(f32[256,2,192]{0,2,1:T(8,128)} %get-tuple-element.145) | data formatting | bytes 589824 | tf_op jit(solution)/shard_map
  110.2 2.0 %fusion.11 = f32[2,256,2048]{2,1,0:T(8,128)S(1)} fusion(bf16[2048,2,256]{0,2,1:T(8,128)(2,1)} %bitcast.31, bf16[256,2,192]{2,0,1:T(8,128)(2,1)} %copy.31), kind=kOutput, calls=%fused_computation.11 | convolution fusion | flops 268435456 | bytes 5373952 | tf_op jit(solution)/shard_map/while/body/eval_jaxpr/cond/branch_1_fun/qhd,khd->hqk/dot_general | solution.py:69
  112.6 1.3 fusion.24
  114.7 0.9 copy-done.1
  115.5 0.9 fusion.7
  116.4 0.8 copy_bitcast_fusion.att_ref
  117.3 22.4 %project_out.1 = bf16[64,4096]{1,0:T(8,128)(2,1)} custom-call(f32[256,256]{1,0:T(8,128)} %recurrent.1.rec_ref, f32[256,256]{1,0:T(8,128)} %copy_bitcast_fusion.att_ref, f32[1,256]{1,0:T(1,128)} %bitcast.38, f32[1,256]{1,0:T(1,128)} %bitcast.39, bf16[256,4096]{1,0:T(8,128)(2,1)} %wrec_ref.1, bf16[256,4096]{1,0:T(8,128)(2,1)} %watt_ref.1, f32[1,4096]{1,0:T(1,128)} %bitcast.35), custom_call_target="tpu_custom_call" | custom-call | flops 1073741824 | bytes 8000000 | tf_op jit(solution)/shard_map/project_out/pallas_call | solution.py:302
  139.7 1.9 %copy.43 = bf16[64,4096]{1,0:T(8,128)(2,1)} copy(bf16[64,4096]{1,0:T(8,128)(2,1)} %project_out.1) | data formatting | bytes 1048576
  (39 shorter events, 2.1 us)
Async XLA Ops:
  6.5 36.7 %copy-start = (bf16[4096,384]{1,0:T(8,128)(2,1)S(1)}, bf16[4096,384]{1,0:T(8,128)(2,1)}, u32[]{:S(2)}) copy-start(bf16[4096,384]{1,0:T(8,128)(2,1)} %param.30) | copy-start | bytes 9437188
  6.5 27.7 %all-gather.3.cloned.1.call-start = ((), (), s32[]{:S(2)}) async-start(), calls=%async_computation | async-start | bytes 2621440 | tf_op jit(solution)/shard_map/all_gather | solution.py:359
  7.3 97.1 %all-gather.5.cloned.1.call-start = ((), (), s32[]{:S(2)}) async-start(), calls=%async_computation.1 | async-start | bytes 2359296 | tf_op jit(solution)/shard_map/all_gather | solution.py:402
  36.3 4.3 %copy-start.4 = (bf16[512,512]{1,0:T(8,128)(2,1)S(1)}, bf16[512,512]{1,0:T(8,128)(2,1)}, u32[]{:S(2)}) copy-start(bf16[512,512]{1,0:T(8,128)(2,1)} %param.34) | copy-start | bytes 1572868
  36.3 4.3 %copy-start.5 = (f32[512]{0:T(512)S(1)}, f32[512]{0:T(512)}, u32[]{:S(2)}) copy-start(f32[512]{0:T(512)} %param.33) | copy-start | bytes 6148
  36.3 5.4 %copy-start.6 = (f32[256]{0:T(256)S(1)}, f32[256]{0:T(256)}, u32[]{:S(2)}) copy-start(f32[256]{0:T(256)} %param.23) | copy-start | bytes 3076
  36.3 6.2 %copy-start.7 = (f32[256]{0:T(256)S(1)}, f32[256]{0:T(256)}, u32[]{:S(2)}) copy-start(f32[256]{0:T(256)} %param.29) | copy-start | bytes 3076
  36.4 6.9 %copy-start.9 = (f32[4096]{0:T(1024)S(1)}, f32[4096]{0:T(1024)}, u32[]{:S(2)}) copy-start(f32[4096]{0:T(1024)} %param.22) | copy-start | bytes 49156
  48.8 4.0 %copy-start.2 = (bf16[256,4096]{1,0:T(8,128)(2,1)S(1)}, bf16[256,4096]{1,0:T(8,128)(2,1)}, u32[]{:S(2)}) copy-start(bf16[256,4096]{1,0:T(8,128)(2,1)} %all-gather.3.cloned.1.call-done) | copy-start | bytes 6291460
  48.8 4.0 %copy-start.8 = (bf16[4096,256]{1,0:T(8,128)(2,1)S(1)}, bf16[4096,256]{1,0:T(8,128)(2,1)}, u32[]{:S(2)}) copy-start(bf16[4096,256]{1,0:T(8,128)(2,1)} %param.24) | copy-start | bytes 6291460
  110.2 2.4 %copy-start.3 = (bf16[2048,64]{0,1:T(8,128)(2,1)S(1)}, bf16[2048,64]{0,1:T(8,128)(2,1)}, u32[]{:S(2)}) copy-start(bf16[2048,64]{0,1:T(8,128)(2,1)} %get-tuple-element.125) | copy-start | bytes 786436 | tf_op jit(solution)/shard_map/while/body/eval_jaxpr/cond
  113.9 1.6 %copy-start.1 = (bf16[2048,512]{0,1:T(8,128)(2,1)S(1)}, bf16[2048,512]{0,1:T(8,128)(2,1)}, u32[]{:S(2)}) copy-start(bf16[2048,512]{0,1:T(8,128)(2,1)} %copy.30) | copy-start | bytes 6291460 | tf_op jit(solution)/shard_map/while/body/eval_jaxpr/cond
Sparse Core Ops, SparseCore 0:
  8.9 25.2 all-gather.2
  41.8 52.3 all-gather.4

commit v3 on v2

--- a/solution.py
+++ b/solution.py
@@ -16,27 +16,6 @@
 EPS = 1e-06
 RATE_C = 8.0
 THETA = 10000.0
-span_limit = 2048
-
-
-def passed_along(block, axis, distance):
-    devices = range(lax.axis_size(axis))
-    route = [(i - distance, i) for i in devices if i - distance in devices]
-    return lax.ppermute(block, axis, route)
-
-
-def entering(value, axis, join, neutral):
-    count, mine = (lax.axis_size(axis), lax.axis_index(axis))
-    pieces = jax.tree.map(lambda part: lax.all_gather(part, axis), value)
-    subtotal = jax.tree.map(
-        lambda part, zero: jnp.full_like(part, 0) + jnp.asarray(zero, part.dtype), value, neutral
-    )
-
-    def step(position, subtotal):
-        longer = join(subtotal, jax.tree.map(lambda part: part[position], pieces))
-        return jax.tree.map(lambda new, old: jnp.where(position < mine, new, old), longer, subtotal)
-
-    return lax.fori_loop(0, count - 1, step, subtotal)
 
 
 def rms_inverse(values):
@@ -57,32 +36,6 @@
     places = (offset + jnp.arange(length)).astype(jnp.float32)
     turned = places[:, None] * frequency[None, :]
     return (jnp.cos(turned), jnp.sin(turned))
-
-
-def combine_steps(earlier, later):
-    return (earlier[0] * later[0], later[0] * earlier[1] + later[1])
-
-
-def attend_block(state_now, query_nope, query_rope, places, keys_nope, key_rope, values, key_root):
-    maxima, totals, accumulated = state_now
-    scaling = 1.0 / math.sqrt(query_nope.shape[-1] + query_rope.shape[-1])
-    scores = jnp.einsum("qhd,khd->hqk", query_nope, keys_nope, preferred_element_type=jnp.float32)
-    scores = scores + jnp.einsum(
-        "qhd,kd->hqk", query_rope, key_rope, preferred_element_type=jnp.float32
-    )
-    scores = scores * scaling
-    key_places = key_root + jnp.arange(keys_nope.shape[0])
-    visible = key_places[None, :] <= places[:, None]
-    scores = jnp.where(visible[None], scores, -jnp.inf)
-    largest = jnp.maximum(maxima, jnp.max(scores, axis=-1))
-    anchor = jnp.where(largest == -jnp.inf, 0.0, largest)
-    weights = jnp.exp(scores - anchor[..., None])
-    shrink = jnp.exp(maxima - anchor)
-    totals = totals * shrink + jnp.sum(weights, axis=-1)
-    accumulated = accumulated * shrink[..., None] + jnp.einsum(
-        "hqk,khd->hqd", weights.astype(jnp.bfloat16), values, preferred_element_type=jnp.float32
-    )
-    return (largest, totals, accumulated)
 
 
 MESH = pl.DeviceIdType.MESH
@@ -329,6 +282,171 @@
     )(rec_out, att_out, rec_gain[None, :], att_gain[None, :], w_out_rec, w_out_att, post_gain[None, :])
 
 
+def attend_kernel(
+    n, m, q_ref, lat_ref, wexp_ref, out_ref,
+    buf, peak, total, accum, p_s, p_r, y_s, y_r, c_s, c_r,
+):
+    me, tp = lax.axis_index("sp"), lax.axis_index("tp")
+    core, group, groups = lax.rem(tp, 2), tp // 2, m // 2
+    partner = group * 2 + (1 - core)
+    pieces, block, wide = lat_ref.shape
+    rows = pieces * block
+    latent = wexp_ref.shape[0]
+    heads = wexp_ref.shape[1] // (NOPE + VDIM)
+    scaling = 1.0 / math.sqrt(NOPE + ROPE)
+    barrier = pltpu.get_barrier_semaphore()
+    for d in range(1, n):
+        pl.semaphore_signal(
+            barrier, inc=1, device_id={"sp": lax.rem(me + d, n)}, device_id_type=MESH
+        )
+    for e in range(1, groups):
+        pl.semaphore_signal(
+            barrier, inc=1, device_id={"tp": lax.rem(group + e, groups) * 2 + core},
+            device_id_type=MESH,
+        )
+    pl.semaphore_signal(barrier, inc=1, device_id={"tp": partner}, device_id_type=MESH)
+    pl.semaphore_wait(barrier, n - 1 + groups)
+
+    def ahead(d):
+        return pltpu.make_async_remote_copy(
+            src_ref=lat_ref.at[tp], dst_ref=buf.at[d, tp], send_sem=p_s.at[d], recv_sem=p_r.at[d],
+            device_id={"sp": lax.rem(me + d, n)}, device_id_type=MESH,
+        )
+
+    def across(d, e):
+        return pltpu.make_async_remote_copy(
+            src_ref=buf.at[d, tp], dst_ref=buf.at[d, tp], send_sem=y_s.at[d, e],
+            recv_sem=y_r.at[d, e], device_id={"tp": lax.rem(group + e, groups) * 2 + core},
+            device_id_type=MESH,
+        )
+
+    def inside(d, e):
+        piece = lax.rem(group - e + groups, groups) * 2 + core
+        return pltpu.make_async_remote_copy(
+            src_ref=buf.at[d, piece], dst_ref=buf.at[d, piece], send_sem=c_s.at[d, e],
+            recv_sem=c_r.at[d, e], device_id={"tp": partner}, device_id_type=MESH,
+        )
+
+    def send_one(d, carry):
+        @pl.when(me + d < n)
+        def _():
+            ahead(d).start()
+
+        return carry
+
+    lax.fori_loop(1, n, send_one, 0)
+
+    def chunk(lat, own):
+        expanded = jnp.dot(
+            lat[:, :latent], wexp_ref[...], preferred_element_type=jnp.float32
+        ).astype(jnp.bfloat16)
+        key_rope = lat[:, latent:]
+        for h in range(heads):
+            base = h * (NOPE + VDIM)
+            keys = jnp.concatenate([expanded[:, base : base + NOPE], key_rope], axis=1)
+            width = keys.shape[1]
+            scores = lax.dot_general(
+                q_ref[:, h * width : (h + 1) * width], keys, (((1,), (1,)), ((), ())),
+                preferred_element_type=jnp.float32,
+            ) * scaling
+            if own:
+                at_row = lax.broadcasted_iota(jnp.int32, scores.shape, 0)
+                at_col = lax.broadcasted_iota(jnp.int32, scores.shape, 1)
+                scores = jnp.where(at_col <= at_row, scores, -jnp.inf)
+            high = jnp.max(scores, axis=1, keepdims=True)
+            if not own:
+                high = jnp.maximum(high, peak[h])
+            weights = jnp.exp(scores - high)
+            added = jnp.sum(weights, axis=1, keepdims=True)
+            mixed = jnp.dot(
+                weights.astype(jnp.bfloat16), expanded[:, base + NOPE : base + NOPE + VDIM],
+                preferred_element_type=jnp.float32,
+            )
+            if not own:
+                shrink = jnp.exp(peak[h] - high)
+                added = added + total[h] * shrink
+                mixed = mixed + accum[h] * shrink
+            peak[h] = high
+            total[h] = added
+            accum[h] = mixed
+
+    chunk(lat_ref[...].reshape(rows, wide), True)
+
+    def step(t, carry):
+        @pl.when(t <= me)
+        def _():
+            ahead(t).wait_recv()
+            for e in range(1, groups):
+                across(t, e).start()
+            inside(t, 0).start()
+
+        @pl.when((t >= 2) & (t - 1 <= me))
+        def _():
+            for e in range(1, groups):
+                across(t - 1, e).wait_recv()
+                inside(t - 1, e).start()
+
+        @pl.when((t >= 3) & (t - 2 <= me))
+        def _():
+            for e in range(groups):
+                inside(t - 2, e).wait_recv()
+            chunk(buf[t - 2].reshape(rows, wide), False)
+
+        return carry
+
+    lax.fori_loop(1, n + 2, step, 0)
+    for h in range(heads):
+        out_ref[:, h * VDIM : (h + 1) * VDIM] = accum[h] / total[h]
+
+    def finish(d, carry):
+        @pl.when(me + d < n)
+        def _():
+            ahead(d).wait_send()
+
+        @pl.when(d <= me)
+        def _():
+            for e in range(1, groups):
+                across(d, e).wait_send()
+            for e in range(groups):
+                inside(d, e).wait_send()
+
+        return carry
+
+    lax.fori_loop(1, n, finish, 0)
+
+
+def attend(query, latent_rope, w_expand):
+    n, m = lax.axis_size("sp"), lax.axis_size("tp")
+    rows, wide = latent_rope.shape
+    heads = w_expand.shape[1] // (NOPE + VDIM)
+    vmem = pl.BlockSpec(memory_space=pltpu.VMEM)
+    dma = pltpu.SemaphoreType.DMA
+    block = rows // m
+    return pl.pallas_call(
+        functools.partial(attend_kernel, n, m),
+        out_shape=jax.ShapeDtypeStruct((rows, heads * VDIM), jnp.float32),
+        in_specs=[vmem] * 3,
+        out_specs=vmem,
+        scratch_shapes=[
+            pltpu.VMEM((n, m, block, wide), jnp.bfloat16),
+            pltpu.VMEM((heads, rows, 1), jnp.float32),
+            pltpu.VMEM((heads, rows, 1), jnp.float32),
+            pltpu.VMEM((heads, rows, VDIM), jnp.float32),
+            dma((n,)),
+            dma((n,)),
+            dma((n, m // 2)),
+            dma((n, m // 2)),
+            dma((n, m // 2)),
+            dma((n, m // 2)),
+        ],
+        compiler_params=pltpu.CompilerParams(collective_id=2, has_side_effects=True),
+        cost_estimate=pl.CostEstimate(
+            flops=2_000_000_000, bytes_accessed=4_000_000, transcendentals=0
+        ),
+        name="attend",
+    )(query, latent_rope.reshape(m, block, wide), w_expand)
+
+
 def shards(
     tokens,
     pre_gain,
@@ -354,8 +472,6 @@
     model_width = w_rec_in.shape[0]
     heads_here = w_query.shape[1] // (NOPE + ROPE)
     first_place = lax.axis_index("sp") * row_count
-    places = first_place + jnp.arange(row_count)
-    last_place = first_place + row_count - 1
     piece_wide = lax.all_gather(tokens, "tp", axis=1, tiled=True).astype(jnp.float32)
     piece_low = (piece_wide * pre_gain).astype(jnp.bfloat16)
 
@@ -385,53 +501,18 @@
     )
     cosine, sine_part = angles(row_count, first_place, ROPE)
     query_heads = query_raw.reshape(row_count, heads_here, NOPE + ROPE)
-    query_nope = query_heads[:, :, :NOPE].astype(jnp.bfloat16)
-    query_rope = rotate(query_heads[:, :, NOPE:], cosine[:, None, :], sine_part[:, None, :]).astype(
-        jnp.bfloat16
+    low = jnp.bfloat16
+    query_rope = rotate(query_heads[:, :, NOPE:], cosine[:, None, :], sine_part[:, None, :])
+    fill = NOPE - ROPE
+    query = jnp.concatenate(
+        [query_heads[:, :, :NOPE], query_rope, jnp.zeros((row_count, heads_here, fill))], axis=-1
+    ).astype(low)
+    own_latent = (latent_raw * rms_inverse(latent_raw) * latent_gain).astype(low)
+    rope_key = rotate(rope_raw, cosine, sine_part).astype(low)
+    latent_rope = jnp.concatenate(
+        [own_latent, rope_key, jnp.zeros((row_count, fill), low)], axis=-1
     )
-    own_latent = (latent_raw * rms_inverse(latent_raw) * latent_gain).astype(jnp.bfloat16)
-    rope_key = rotate(rope_raw, cosine, sine_part).astype(jnp.bfloat16)
-    start_state = (
-        jnp.full((heads_here, row_count), -jnp.inf, jnp.float32),
-        jnp.zeros((heads_here, row_count), jnp.float32),
-        jnp.zeros((heads_here, row_count, VDIM), jnp.float32),
-    )
-    expanded_local = jnp.dot(own_latent, w_expand, preferred_element_type=jnp.float32).astype(
-        jnp.bfloat16
-    )
-    key_source = lax.all_gather(expanded_local, "sp", axis=0, tiled=True)
-    rope_source = lax.all_gather(rope_key, "sp", axis=0, tiled=True)
-    total_rows = key_source.shape[0]
-    key_span = math.gcd(total_rows, span_limit)
-
-    def one_span(span_index, state_inner):
-        key_root = span_index * key_span
-
-        def compute(state_deep):
-            source_rows = lax.dynamic_slice_in_dim(key_source, span_index * key_span, key_span, 0)
-            rope_rows = lax.dynamic_slice_in_dim(rope_source, span_index * key_span, key_span, 0)
-            expanded = source_rows
-            expanded = expanded.reshape(key_span, heads_here, NOPE + VDIM)
-            return attend_block(
-                state_deep,
-                query_nope,
-                query_rope,
-                places,
-                expanded[:, :, :NOPE],
-                rope_rows,
-                expanded[:, :, NOPE:],
-                key_root,
-            )
-
-        def keep_state(state_deep):
-            return state_deep
-
-        return lax.cond(key_root <= last_place, compute, keep_state, state_inner)
-
-    maxima, totals, accumulated = lax.fori_loop(0, total_rows // key_span, one_span, start_state)
-    att_out = (
-        (accumulated / totals[..., None]).transpose(1, 0, 2).reshape(row_count, heads_here * VDIM)
-    )
+    att_out = attend(query.reshape(row_count, heads_here * 2 * NOPE), latent_rope, w_expand)
     return project_out(rec_out, att_out, rec_gain, att_gain, w_out_rec, w_out_att, post_gain)
 
 

time: 149 us -> 135 us (0.906)
  Pallas kernels: 35.3 us -> 70 us
  blocking collectives: 33.8 us -> 0 us
  matrix products: 20.9 us -> 14.6 us
  waiting for transfers between devices: 27.6 us -> 22.6 us
  local copies, waits for them, and re-layouts: 11.3 us -> 6.92 us
  other arithmetic: 5.78 us -> 7.52 us
    all_gather x1 -> x0, blocking collectives: 33.8 us -> none  [shards(): rope_source = lax.all_gather(rope_key, 'sp', axis=0, tiled=True)]
    pallas_call x0 -> x1, Pallas kernels: none -> 17.8 us  [attend(): pl.pallas_call(functools.partial(attend_kernel, n, m), out_shape=jax.Shap...]
    pallas_call x1, Pallas kernels: 12.9 us -> 29.9 us  [recurrent(): pl.pallas_call(functools.partial(rec_kernel, n), out_shape=jax.ShapeDtype...]
    another operation x2, local copies, waits for them, and re-layouts: 5.81 us -> 0.24 us
    dot_general x4 -> x0, matrix products: 5.32 us -> none  [the longest x1 2.03 us: attend_block(): jnp.einsum('qhd,khd->hqk', query_nope, keys_nope, preferred_element_type=...]
    all_gather x1, waiting for transfers between devices: 26.9 us -> 21.9 us  [shards(): lax.all_gather(tokens, 'tp', axis=1, tiled=True).astype(jnp.float32)]
  transfers between devices with their start and end apart: 2 -> 1, of which waited for: 1 -> 1; matrix products, arithmetic and copies ran while one was open for 11% -> 4% of each run, Pallas kernels for 9% -> 0%
where the time goes in v3:
time: 135 us
  Pallas kernels  70 us (52%)
  waiting for transfers between devices  22.6 us (17%)
  matrix products  14.6 us (11%)
  between operations  13.6 us (10%)
  other arithmetic  7.52 us (6%)
  local copies, waits for them, and re-layouts  6.92 us (5%)
    pallas_call x1, Pallas kernels, recurrent(): pl.pallas_call(functools.partial(rec_kernel, n), out_shape=jax.ShapeDtype...  29.9 us
    pallas_call x1, Pallas kernels, project_out(): pl.pallas_call(functools.partial(out_kernel, n), out_shape=jax.ShapeDtype...  22.2 us
    all_gather x1, waiting for transfers between devices, shards(): lax.all_gather(tokens, 'tp', axis=1, tiled=True).astype(jnp.float32)  21.9 us
    pallas_call x1, Pallas kernels, attend(): pl.pallas_call(functools.partial(attend_kernel, n, m), out_shape=jax.Shap...  17.8 us
    dot_general x5, matrix products, accumulate(): return jnp.dot(source, weight, preferred_element_type=jnp.float32)  14.6 us
  transfers between devices with their start and end apart: 1, of which 1 were waited for; matrix products, arithmetic and copies ran while one was open for 4% of the time, Pallas kernels for 0%

profile of v3, /device:TPU:0, one launch (start us, length us, event | category | flops | bytes accessed | tf_op | source)
XLA Modules:
  0.0 135.1 jit_solution(11275745012084094352)
XLA Ops:
  6.5 0.7 all-gather.2.cloned.1.call-update
  7.3 0.6 pad.7.clone
  7.9 0.7 pad.3.clone
  8.5 1.5 %copy.27.rate_ref = f32[256,1]{1,0:T(8,128)} copy(f32[256,1]{0,1:T(1,128)} %bitcast.19) | data formatting | bytes 2048 | tf_op jit(solution)/shard_map/broadcast_in_dim | solution.py:499
  10.0 0.6 negate_power_fusion
  10.6 0.5 add_convert_fusion.2
  11.1 1.2 compare_select_fusion
  12.4 21.9 %all-gather.2.cloned.1.call-done = bf16[256,4096]{1,0:T(8,128)(2,1)} async-done(((bf16[256,1024]{1,0:T(8,128)(2,1)}), bf16[256,4096]{1,0:T(8,128)(2,1)}) %all-gather.2.cloned.1.call-update) | async-done | bytes 2097168 | tf_op jit(solution)/shard_map/all_gather | solution.py:475
  34.2 2.2 %fusion = f32[256]{0:T(256)S(1)} fusion(bf16[256,4096]{1,0:T(8,128)(2,1)} %all-gather.2.cloned.1.call-done), kind=kLoop, calls=%fused_computation.2 | loop fusion | flops 3145472 | bytes 2098176 | tf_op jit(solution)/shard_map/reduce_sum | solution.py:481
  36.5 2.1 %convolution_multiply_fusion.1 = f32[256,384]{1,0:T(8,128)} fusion(bf16[4096,384]{1,0:T(8,128)(2,1)S(1)} %copy-done, bf16[256,4096]{1,0:T(8,128)(2,1)S(1)} %copy-done.1, f32[4096]{0:T(1024)S(1)} %copy-done.12, f32[256]{0:T(256)S(1)} %add_rsqrt_fusion.1), kind=kOutput, calls=%fused_computation.5 | convolution fusion | flops 808550400 | bytes 5653504 | tf_op jit(solution)/shard_map/dot_general | solution.py:479
  38.6 1.2 copy.28
  39.8 2.5 %convolution_multiply_fusion.4 = f32[256,64]{0,1:T(8,128)S(1)} fusion(bf16[4096,64]{0,1:T(8,128)(2,1)} %param.30, bf16[256,4096]{1,0:T(8,128)(2,1)} %all-gather.2.cloned.1.call-done, f32[4096]{0:T(1024)} %param.20, f32[256]{0:T(256)S(1)} %add_rsqrt_fusion.1), kind=kOutput, calls=%fused_computation.9 | convolution fusion | flops 137379840 | bytes 2704384 | tf_op jit(solution)/shard_map/dot_general | solution.py:479
  42.3 0.8 subtract_convert_fusion.1
  43.2 0.8 copy.32.q_ref
  44.1 4.9 %multiply_reduce_fusion = (f32[256]{0:T(256)S(1)}, f32[256,512]{1,0:T(8,128)}) fusion(bf16[4096,512]{1,0:T(8,128)(2,1)} %param.29, bf16[256,4096]{1,0:T(8,128)(2,1)} %all-gather.2.cloned.1.call-done, f32[4096]{0:T(1024)} %param.20, f32[256]{0:T(256)} %copy-done.7), kind=kOutput, calls=%fused_computation.11 | convolution fusion | flops 1077280512 | bytes 6834176 | tf_op jit(solution)/shard_map/dot_general | solution.py:479
  49.1 0.1 copy.31
  49.2 1.2 multiply_convert_fusion
  50.4 0.8 maximum_maximum_fusion
  51.2 17.8 %attend.1.att_ref = f32[256,256]{1,0:T(8,128)} custom-call(bf16[256,512]{1,0:T(8,128)(2,1)} %copy.32.q_ref, bf16[4,64,640]{2,1,0:T(8,128)(2,1)} %bitcast.16, bf16[512,512]{1,0:T(8,128)(2,1)} %wexp_ref.1), custom_call_target="tpu_custom_call" | custom-call | flops 2000000000 | bytes 4000000 | tf_op jit(solution)/shard_map/attend/pallas_call | solution.py:425
  69.1 3.8 %convolution_multiply_fusion.2.gate_ref = f32[256,256]{1,0:T(8,128)} fusion(bf16[4096,256]{1,0:T(8,128)(2,1)} %param.23, bf16[256,4096]{1,0:T(8,128)(2,1)} %all-gather.2.cloned.1.call-done, f32[4096]{0:T(1024)S(1)} %copy-done.13, f32[256]{0:T(256)S(1)} %copy-done.8), kind=kOutput, calls=%fused_computation.6 | convolution fusion | flops 540082176 | bytes 4473856 | tf_op jit(solution)/shard_map/dot_general | solution.py:479
  72.9 1.4 %fusion.2.rec_ref = bf16[256,256]{1,0:T(8,128)(2,1)} fusion(bf16[4096,256]{1,0:T(8,128)(2,1)S(1)} %copy-done.11, bf16[256,4096]{1,0:T(8,128)(2,1)S(1)} %copy-done.2, f32[4096]{0:T(1024)S(1)} %copy-done.13, f32[256]{0:T(256)S(1)} %copy-done.8), kind=kOutput, calls=%fused_computation.8 | convolution fusion | flops 540147712 | bytes 4342784 | tf_op jit(solution)/shard_map/dot_general | solution.py:479
  74.3 29.9 %recurrent.1.rec_ref = f32[256,256]{1,0:T(8,128)} custom-call(bf16[256,256]{1,0:T(8,128)(2,1)} %fusion.2.rec_ref, f32[4,256]{1,0:T(4,128)} %taps_ref.1, bf16[2,128,128]{2,1,0:T(8,128)(2,1)} %rmap_ref.1, bf16[2,128,128]{2,1,0:T(8,128)(2,1)} %imap_ref.1, f32[1,256]{1,0:T(1,128)} %bitcast.18, f32[256,1]{1,0:T(8,128)} %copy.27.rate_ref, ...), custom_call_target="tpu_custom_call" | custom-call | flops 20000000 | bytes 2000000 | tf_op jit(solution)/shard_map/recurrent/pallas_call | solution.py:128
  104.2 22.2 %project_out.1 = bf16[64,4096]{1,0:T(8,128)(2,1)} custom-call(f32[256,256]{1,0:T(8,128)} %recurrent.1.rec_ref, f32[256,256]{1,0:T(8,128)} %attend.1.att_ref, f32[1,256]{1,0:T(1,128)} %bitcast.20, f32[1,256]{1,0:T(1,128)} %bitcast.21, bf16[256,4096]{1,0:T(8,128)(2,1)} %wrec_ref.1, bf16[256,4096]{1,0:T(8,128)(2,1)} %watt_ref.1, f32[1,4096]{1,0:T(1,128)} %bitcast.17), custom_call_target="tpu_custom_call" | custom-call | flops 1073741824 | bytes 8000000 | tf_op jit(solution)/shard_map/project_out/pallas_call | solution.py:255
  126.4 1.9 %copy.34 = bf16[64,4096]{1,0:T(8,128)(2,1)} copy(bf16[64,4096]{1,0:T(8,128)(2,1)} %project_out.1) | data formatting | bytes 1048576
  (36 shorter events, 0.3 us)
Async XLA Ops:
  6.5 29.9 %copy-start = (bf16[4096,384]{1,0:T(8,128)(2,1)S(1)}, bf16[4096,384]{1,0:T(8,128)(2,1)}, u32[]{:S(2)}) copy-start(bf16[4096,384]{1,0:T(8,128)(2,1)} %param.28) | copy-start | bytes 9437188
  6.5 29.9 %copy-start.12 = (f32[4096]{0:T(1024)S(1)}, f32[4096]{0:T(1024)}, u32[]{:S(2)}) copy-start(f32[4096]{0:T(1024)} %param.20) | copy-start | bytes 49156
  6.5 27.7 %all-gather.2.cloned.1.call-start = ((), (), s32[]{:S(2)}) async-start(), calls=%async_computation | async-start | bytes 2621440 | tf_op jit(solution)/shard_map/all_gather | solution.py:475
  34.2 2.3 %copy-start.1 = (bf16[256,4096]{1,0:T(8,128)(2,1)S(1)}, bf16[256,4096]{1,0:T(8,128)(2,1)}, u32[]{:S(2)}) copy-start(bf16[256,4096]{1,0:T(8,128)(2,1)} %all-gather.2.cloned.1.call-done) | copy-start | bytes 6291460
  36.5 3.3 %copy-start.7 = (f32[256]{0:T(256)}, f32[256]{0:T(256)S(1)}, u32[]{:S(2)}) copy-start(f32[256]{0:T(256)S(1)} %add_rsqrt_fusion.1) | copy-start | bytes 3076
  39.7 2.5 %copy-start.6 = (f32[256]{0:T(256)S(1)}, f32[256]{0:T(256)}, u32[]{:S(2)}) copy-start(f32[256]{0:T(256)} %add_convert_fusion.2) | copy-start | bytes 3076
  39.7 2.5 %copy-start.9 = (f32[32]{0:T(128)S(1)}, f32[32]{0:T(128)}, u32[]{:S(2)}) copy-start(f32[32]{0:T(128)} %negate_power_fusion) | copy-start | bytes 388
  39.7 3.4 %copy-start.10 = (bf16[256]{0:T(256)(128)(2,1)S(1)}, bf16[256]{0:T(256)(128)(2,1)}, u32[]{:S(2)}) copy-start(bf16[256]{0:T(256)(128)(2,1)} %pad.7.clone) | copy-start | bytes 1540
  44.1 4.9 %copy-start.3 = (bf16[256,32]{0,1:T(8,128)(2,1)S(1)}, bf16[256,32]{0,1:T(8,128)(2,1)}, u32[]{:S(2)}) copy-start(bf16[256,32]{0,1:T(8,128)(2,1)} %get-tuple-element.7) | copy-start | bytes 49156
  44.1 5.2 %copy-start.5 = (f32[512]{0:T(512)S(1)}, f32[512]{0:T(512)}, u32[]{:S(2)}) copy-start(f32[512]{0:T(512)} %param.31) | copy-start | bytes 6148
  44.1 6.3 %copy-start.4 = (bf16[640]{0:T(1024)(128)(2,1)S(1)}, bf16[640]{0:T(1024)(128)(2,1)}, u32[]{:S(2)}) copy-start(bf16[640]{0:T(1024)(128)(2,1)} %pad.3.clone) | copy-start | bytes 3844
  51.2 17.8 %copy-start.8 = (f32[256]{0:T(256)S(1)}, f32[256]{0:T(256)}, u32[]{:S(2)}) copy-start(f32[256]{0:T(256)} %copy-done.7) | copy-start | bytes 3076
  51.2 17.8 %copy-start.13 = (f32[4096]{0:T(1024)S(1)}, f32[4096]{0:T(1024)}, u32[]{:S(2)}) copy-start(f32[4096]{0:T(1024)} %param.20) | copy-start | bytes 49156
  69.1 3.8 %copy-start.2 = (bf16[256,4096]{1,0:T(8,128)(2,1)S(1)}, bf16[256,4096]{1,0:T(8,128)(2,1)}, u32[]{:S(2)}) copy-start(bf16[256,4096]{1,0:T(8,128)(2,1)} %all-gather.2.cloned.1.call-done) | copy-start | bytes 6291460
  69.1 3.8 %copy-start.11 = (bf16[4096,256]{1,0:T(8,128)(2,1)S(1)}, bf16[4096,256]{1,0:T(8,128)(2,1)}, u32[]{:S(2)}) copy-start(bf16[4096,256]{1,0:T(8,128)(2,1)} %param.22) | copy-start | bytes 6291460
Sparse Core Ops, SparseCore 0:
  8.9 25.2 all-gather.1

commit v4 on v3

--- a/solution.py
+++ b/solution.py
@@ -16,10 +16,6 @@
 EPS = 1e-06
 RATE_C = 8.0
 THETA = 10000.0
-
-
-def rms_inverse(values):
-    return lax.rsqrt(jnp.mean(values * values, axis=-1, keepdims=True) + EPS)
 
 
 def rotate(values, cosine, sine_part):
@@ -447,6 +443,140 @@
     )(query, latent_rope.reshape(m, block, wide), w_expand)
 
 
+def project_kernel(
+    n, tok_ref, gain_ref, lgain_ref, wrope_ref, w_in, w_gate, w_query, w_latent,
+    rec_ref, gate_ref, query_ref, latent_ref, rope_ref,
+    buf, v_in, v_gate, v_query, v_latent, a_in, a_latent, w_sem, y_s, y_r, c_s, c_r,
+):
+    tp = lax.axis_index("tp")
+    core, group, groups = lax.rem(tp, 2), tp // 2, n // 2
+    partner = group * 2 + (1 - core)
+    parts, sub, depth = tok_ref.shape
+    rows = parts * sub
+    loads = []
+    for i, (src, dst) in enumerate(
+        ((w_in, v_in), (w_gate, v_gate), (w_query, v_query), (w_latent, v_latent))
+    ):
+        loads.append(pltpu.make_async_copy(src, dst, w_sem.at[i]))
+        loads[-1].start()
+    barrier = pltpu.get_barrier_semaphore()
+    for e in range(1, groups):
+        pl.semaphore_signal(
+            barrier, inc=1, device_id={"tp": lax.rem(group + e, groups) * 2 + core},
+            device_id_type=MESH,
+        )
+    pl.semaphore_signal(barrier, inc=1, device_id={"tp": partner}, device_id_type=MESH)
+    pl.semaphore_wait(barrier, groups)
+
+    def origin(e):
+        return lax.rem(group - e + groups, groups) * 2
+
+    def across(e, r):
+        return pltpu.make_async_remote_copy(
+            src_ref=tok_ref.at[r], dst_ref=buf.at[tp, r], send_sem=y_s.at[e, r],
+            recv_sem=y_r.at[e, r], device_id={"tp": lax.rem(group + e, groups) * 2 + core},
+            device_id_type=MESH,
+        )
+
+    def inside(e, r):
+        piece = origin(e) + core
+        return pltpu.make_async_remote_copy(
+            src_ref=tok_ref.at[r] if e == 0 else buf.at[piece, r], dst_ref=buf.at[piece, r],
+            send_sem=c_s.at[e, r], recv_sem=c_r.at[e, r], device_id={"tp": partner},
+            device_id_type=MESH,
+        )
+
+    for e in range(1, groups):
+        for r in range(parts):
+            across(e, r).start()
+    for r in range(parts):
+        inside(0, r).start()
+
+    def multiply(values, piece, first):
+        wide = values.reshape(rows, depth).astype(jnp.float32)
+        scaled = (wide * gain_ref[piece]).astype(jnp.bfloat16)
+        here = pl.ds(pl.multiple_of(piece * depth, depth), depth)
+        for weight, total in (
+            (v_in, a_in), (v_gate, gate_ref), (v_query, query_ref),
+            (v_latent, a_latent), (wrope_ref, rope_ref),
+        ):
+            product = jnp.dot(scaled, weight[here, :], preferred_element_type=jnp.float32)
+            total[...] = product if first else total[...] + product
+        return jnp.sum(wide * wide, axis=1, keepdims=True)
+
+    for load in loads:
+        load.wait()
+    squares = multiply(tok_ref[...], tp, True)
+    for r in range(parts):
+        inside(0, r).wait_recv()
+    squares = squares + multiply(buf[partner], partner, False)
+    for e in range(1, groups):
+        for r in range(parts):
+            across(e, r).wait_recv()
+            inside(e, r).start()
+        squares = squares + multiply(buf[origin(e) + core], origin(e) + core, False)
+        for r in range(parts):
+            inside(e, r).wait_recv()
+        squares = squares + multiply(buf[origin(e) + 1 - core], origin(e) + 1 - core, False)
+    inverse = lax.rsqrt(squares / (depth * n) + EPS)
+    rec_ref[...] = (inverse * a_in[...]).astype(jnp.bfloat16)
+    gate_ref[...] = inverse * gate_ref[...]
+    query_ref[...] = inverse * query_ref[...]
+    rope_ref[...] = inverse * rope_ref[...]
+    latent = inverse * a_latent[...]
+    mean = jnp.mean(latent * latent, axis=1, keepdims=True)
+    latent_ref[...] = (latent * lax.rsqrt(mean + EPS) * lgain_ref[...]).astype(jnp.bfloat16)
+    for r in range(parts):
+        inside(0, r).wait_send()
+        for e in range(1, groups):
+            across(e, r).wait_send()
+            inside(e, r).wait_send()
+
+
+def project_in(tokens, pre_gain, latent_gain, w_rope, w_in, w_gate, w_query, w_latent):
+    n = lax.axis_size("tp")
+    rows, depth = tokens.shape
+    parts = math.gcd(rows // 16, 4)
+    sub = rows // parts
+    low, wide, dma = jnp.bfloat16, jnp.float32, pltpu.SemaphoreType.DMA
+    vmem, anywhere = pl.BlockSpec(memory_space=pltpu.VMEM), pl.BlockSpec(memory_space=pl.ANY)
+
+    def shape(weight, kind):
+        return jax.ShapeDtypeStruct((rows, weight.shape[1]), kind)
+
+    return pl.pallas_call(
+        functools.partial(project_kernel, n),
+        out_shape=(
+            shape(w_in, low), shape(w_gate, wide), shape(w_query, wide),
+            shape(w_latent, low), shape(w_rope, wide),
+        ),
+        in_specs=[vmem] * 4 + [anywhere] * 4,
+        out_specs=(vmem,) * 5,
+        scratch_shapes=[
+            pltpu.VMEM((n, parts, sub, depth), low),
+            pltpu.VMEM(w_in.shape, low),
+            pltpu.VMEM(w_gate.shape, low),
+            pltpu.VMEM(w_query.shape, low),
+            pltpu.VMEM(w_latent.shape, low),
+            pltpu.VMEM((rows, w_in.shape[1]), wide),
+            pltpu.VMEM((rows, w_latent.shape[1]), wide),
+            dma((4,)),
+            dma((n // 2, parts)),
+            dma((n // 2, parts)),
+            dma((n // 2, parts)),
+            dma((n // 2, parts)),
+        ],
+        compiler_params=pltpu.CompilerParams(collective_id=3, has_side_effects=True),
+        cost_estimate=pl.CostEstimate(
+            flops=3_000_000_000, bytes_accessed=14_000_000, transcendentals=0
+        ),
+        name="project_in",
+    )(
+        tokens.reshape(parts, sub, depth), pre_gain.reshape(n, 1, depth), latent_gain[None, :],
+        w_rope, w_in, w_gate, w_query, w_latent,
+    )
+
+
 def shards(
     tokens,
     pre_gain,
@@ -469,27 +599,11 @@
     post_gain,
 ):
     row_count = tokens.shape[0]
-    model_width = w_rec_in.shape[0]
     heads_here = w_query.shape[1] // (NOPE + ROPE)
     first_place = lax.axis_index("sp") * row_count
-    piece_wide = lax.all_gather(tokens, "tp", axis=1, tiled=True).astype(jnp.float32)
-    piece_low = (piece_wide * pre_gain).astype(jnp.bfloat16)
-
-    def accumulate(source, weight):
-        return jnp.dot(source, weight, preferred_element_type=jnp.float32)
-
-    squares = jnp.sum(piece_wide * piece_wide, axis=1, keepdims=True)
-    sum_input = accumulate(piece_low, w_rec_in)
-    sum_gate = accumulate(piece_low, w_rec_gate)
-    sum_query = accumulate(piece_low, w_query)
-    sum_latent = accumulate(piece_low, w_latent)
-    sum_rope = accumulate(piece_low, w_rope_key)
-    inverse = lax.rsqrt(squares / model_width + EPS)
-    rec_input = (inverse * sum_input).astype(jnp.bfloat16)
-    gate_value = inverse * sum_gate
-    query_raw = inverse * sum_query
-    latent_raw = inverse * sum_latent
-    rope_raw = inverse * sum_rope
+    rec_input, gate_value, query_raw, own_latent, rope_raw = project_in(
+        tokens, pre_gain, latent_gain, w_rope_key, w_rec_in, w_rec_gate, w_query, w_latent
+    )
     rec_out = recurrent(
         rec_input,
         conv_taps,
@@ -507,7 +621,6 @@
     query = jnp.concatenate(
         [query_heads[:, :, :NOPE], query_rope, jnp.zeros((row_count, heads_here, fill))], axis=-1
     ).astype(low)
-    own_latent = (latent_raw * rms_inverse(latent_raw) * latent_gain).astype(low)
     rope_key = rotate(rope_raw, cosine, sine_part).astype(low)
     latent_rope = jnp.concatenate(
         [own_latent, rope_key, jnp.zeros((row_count, fill), low)], axis=-1

time: 135 us -> 102 us (0.76)
  waiting for transfers between devices: 22.6 us -> 0 us
  Pallas kernels: 70 us -> 91.4 us
  matrix products: 14.6 us -> 0 us
  between operations: 13.6 us -> 0.12 us
  other arithmetic: 7.52 us -> 3.15 us
    all_gather x1 -> x0, waiting for transfers between devices: 21.9 us -> none  [shards(): lax.all_gather(tokens, 'tp', axis=1, tiled=True).astype(jnp.float32)]
    pallas_call x0 -> x1, Pallas kernels: none -> 20.7 us  [project_in(): pl.pallas_call(functools.partial(project_kernel, n), out_shape=(shape(w_i...]
    dot_general x5 -> x0, matrix products: 14.6 us -> none  [accumulate(): return jnp.dot(source, weight, preferred_element_type=jnp.float32)]
    unnamed x29 -> x8, local copies, waits for them, and re-layouts: 1.93 us -> 4.24 us
    reduce_sum x1 -> x0, other arithmetic: 2.23 us -> none  [shards(): squares = jnp.sum(piece_wide * piece_wide, axis=1, keepdims=True)]
  transfers between devices with their start and end apart: 1 -> 0, of which waited for: 1 -> 0; matrix products, arithmetic and copies ran while one was open for 4% -> 0% of each run, Pallas kernels for 0% -> 0%
where the time goes in v4:
time: 102 us
  Pallas kernels  91.4 us (90%)
  local copies, waits for them, and re-layouts  7.36 us (7%)
  other arithmetic  3.15 us (3%)
    pallas_call x1, Pallas kernels, recurrent(): pl.pallas_call(functools.partial(rec_kernel, n), out_shape=jax.ShapeDtype...  29.9 us
    pallas_call x1, Pallas kernels, project_out(): pl.pallas_call(functools.partial(out_kernel, n), out_shape=jax.ShapeDtype...  22.7 us
    pallas_call x1, Pallas kernels, project_in(): pl.pallas_call(functools.partial(project_kernel, n), out_shape=(shape(w_i...  20.7 us
    pallas_call x1, Pallas kernels, attend(): pl.pallas_call(functools.partial(attend_kernel, n, m), out_shape=jax.Shap...  18.1 us
    unnamed x8, local copies, waits for them, and re-layouts  4.24 us

profile of v4, /device:TPU:0, one launch (start us, length us, event | category | flops | bytes accessed | tf_op | source)
XLA Modules:
  0.0 102.1 jit_solution(11233797318437494924)
XLA Ops:
  0.0 2.4 %copy.27.wrope_ref = bf16[4096,64]{1,0:T(8,128)(2,1)} copy(bf16[4096,64]{0,1:T(8,128)(2,1)} %param.30) | data formatting | bytes 1048576 | tf_op args[11]
  2.4 20.7 %project_in.1 = (bf16[256,256]{1,0:T(8,128)(2,1)}, f32[256,256]{1,0:T(8,128)}, f32[256,384]{1,0:T(8,128)}, bf16[256,512]{1,0:T(8,128)(2,1)}, f32[256,64]{1,0:T(8,128)}) custom-call(bf16[4,64,1024]{2,1,0:T(8,128)(2,1)} %bitcast.14, f32[4,1,1024]{2,1,0:T(1,128)} %bitcast.16, f32[1,512]{1,0:T(1,128)} %bitcast.19, bf16[4096,64]{1,0:T(8,128)(2,1)} %copy.27.wrope_ref, ...), custom_call_target="tpu_custom_call" | custom-call | flops 3000000000 | bytes 14000000 | tf_op jit(solution)/shard_map/project_in/pallas_call | solution.py:547
  23.1 0.0 copy-start
  23.1 1.6 %subtract_convert_fusion = (bf16[256,32]{1,0:T(8,128)(2,1)S(1)}, bf16[256,32]{1,0:T(8,128)(2,1)S(1)}, f32[256,32]{1,0:T(8,128)S(1)}, f32[256,32]{1,0:T(8,128)S(1)}) fusion(f32[256,64]{1,0:T(8,128)} %get-tuple-element.14, f32[256]{0:T(256)S(1)} %add_convert_fusion.2, f32[32]{0:T(128)S(1)} %negate_power_fusion), kind=kLoop, calls=%fused_computation.6 | loop fusion | flops 73728 | bytes 164992 | tf_op jit(solution)/shard_map/convert
  24.7 0.1 copy.31
  24.8 0.1 copy.32
  24.8 1.2 %copy.29 = f32[256,384]{0,1:T(8,128)S(1)} copy(f32[256,384]{1,0:T(8,128)} %get-tuple-element.12) | data formatting | bytes 786432 | tf_op jit(solution)/shard_map/project_in/pallas_call | solution.py:547
  26.1 0.1 pad.7.clone
  26.2 0.1 maximum_maximum_fusion.1
  26.3 0.8 copy.34.q_ref
  27.1 0.1 pad.3.clone
  27.2 0.0 copy-done
  27.2 0.8 maximum_maximum_fusion
  28.0 0.0 copy-start.1
  28.0 0.0 copy-start.2
  28.0 18.1 %attend.1.att_ref = f32[256,256]{1,0:T(8,128)} custom-call(bf16[256,512]{1,0:T(8,128)(2,1)} %copy.34.q_ref, bf16[4,64,640]{2,1,0:T(8,128)(2,1)} %bitcast.15, bf16[512,512]{1,0:T(8,128)(2,1)} %wexp_ref.1), custom_call_target="tpu_custom_call" | custom-call | flops 2000000000 | bytes 4000000 | tf_op jit(solution)/shard_map/attend/pallas_call | solution.py:421
  46.1 0.0 copy-done.1
  46.1 0.8 copy.28.rate_ref
  46.9 0.0 copy-done.2
  46.9 0.6 compare_select_fusion
  47.5 29.9 %recurrent.1.rec_ref = f32[256,256]{1,0:T(8,128)} custom-call(bf16[256,256]{1,0:T(8,128)(2,1)} %get-tuple-element.10.rec_ref, f32[4,256]{1,0:T(4,128)} %taps_ref.1, bf16[2,128,128]{2,1,0:T(8,128)(2,1)} %rmap_ref.1, bf16[2,128,128]{2,1,0:T(8,128)(2,1)} %imap_ref.1, f32[1,256]{1,0:T(1,128)} %bitcast.18, f32[256,1]{1,0:T(8,128)} %copy.28.rate_ref, ...), custom_call_target="tpu_custom_call" | custom-call | flops 20000000 | bytes 2000000 | tf_op jit(solution)/shard_map/recurrent/pallas_call | solution.py:124
  77.4 22.7 %project_out.1 = bf16[64,4096]{1,0:T(8,128)(2,1)} custom-call(f32[256,256]{1,0:T(8,128)} %recurrent.1.rec_ref, f32[256,256]{1,0:T(8,128)} %attend.1.att_ref, f32[1,256]{1,0:T(1,128)} %bitcast.21, f32[1,256]{1,0:T(1,128)} %bitcast.22, bf16[256,4096]{1,0:T(8,128)(2,1)} %wrec_ref.1, bf16[256,4096]{1,0:T(8,128)(2,1)} %watt_ref.1, f32[1,4096]{1,0:T(1,128)} %bitcast.17), custom_call_target="tpu_custom_call" | custom-call | flops 1073741824 | bytes 8000000 | tf_op jit(solution)/shard_map/project_out/pallas_call | solution.py:251
  100.2 1.9 %copy.36 = bf16[64,4096]{1,0:T(8,128)(2,1)} copy(bf16[64,4096]{1,0:T(8,128)(2,1)} %project_out.1) | data formatting | bytes 1048576
  (5 shorter events, 0.1 us)
Async XLA Ops:
  23.1 4.1 %copy-start = (bf16[256,512]{1,0:T(8,128)(2,1)S(1)}, bf16[256,512]{1,0:T(8,128)(2,1)}, u32[]{:S(2)}) copy-start(bf16[256,512]{1,0:T(8,128)(2,1)} %get-tuple-element.13) | copy-start | bytes 786436
  28.0 18.1 %copy-start.1 = (f32[256]{0:T(256)S(1)}, f32[256]{0:T(256)}, u32[]{:S(2)}) copy-start(f32[256]{0:T(256)} %param.21) | copy-start | bytes 3076
  28.0 18.9 %copy-start.2 = (f32[256]{0:T(256)S(1)}, f32[256]{0:T(256)}, u32[]{:S(2)}) copy-start(f32[256]{0:T(256)} %param.27) | copy-start | bytes 3076
